TPU v7x, 128 devices: a whole 4x4x4 slice. The times are simulated.
128 devices in a mesh: gr: 2 (over z_hi), fs: 32 (over z_lo, y, x), tp: 2 (over core).
Axes of the slice: x: 4, y: 4, z: 4 (z_hi: 2, z_lo: 2; z = z_hi * 2 + z_lo), core: 2. Of those that a mesh axis runs over, the one named last changes fastest.
Arguments:
- tokens: bfloat16 [65536, 3072], P(('gr', 'fs')), may hold values from -6 to 6
- norm_gain: float32 [3072], P(('gr', 'fs')), may hold values from 0.1 to 1.9
- gate_weight: float32 [32, 3072, 768], P(None, ('gr', 'fs'), 'tp'), may hold values from -0.109375 to 0.109375
- up_weight: float32 [32, 3072, 768], P(None, ('gr', 'fs'), 'tp'), may hold values from -0.109375 to 0.109375
- down_weight: float32 [32, 3072, 768], P(None, ('gr', 'fs'), 'tp'), may hold values from -0.21875 to 0.21875
- group_pick: int32 [65536], P(('gr', 'fs')), may hold values from 0 to 3, as said below
- expert_pick: int32 [65536, 2], P(('gr', 'fs')), may hold values from 0 to 7, as said below
- route_weight: float32 [65536, 2], P(('gr', 'fs')), may hold values from 0.1 to 1
Outputs:
- combined: bfloat16 [65536, 3072], P(('gr', 'fs'), 'tp')
- gate_served: bfloat16 [32, 3072, 768], P('fs', None, 'tp')
- up_served: bfloat16 [32, 3072, 768], P('fs', None, 'tp')
- down_served: bfloat16 [32, 3072, 768], P('fs', None, 'tp')
Inputs may be any that keep to these rules, and one draw needn't show every extreme that they name: `group_pick`: in each aligned block of 1024 rows every group is picked by the same number of rows. `expert_pick`: the 2 entries of a row differ. In each aligned block of 1024 rows, every expert (group and number together) is named exactly 64 times.
All inputs are finite; a program needn't handle non-finite values.
Results may differ from a plain program's by a relative error of at most 0.0092.
Values may be sent and summed in bfloat16 or wider, within the bound.
A program may use at most 128 MiB of HBM per device.

v0:
```python
import jax
import jax.numpy as jnp
from jax import lax
from jax.sharding import PartitionSpec as P

GROUPS = 4


EPS = 1e-06


def sent_together(arrays, axis, split_dim, concat_dim, along):
    both = jnp.concatenate(arrays, axis=along)
    result, at, gathered = (
        lax.all_to_all(both, axis, split_axis=split_dim, concat_axis=concat_dim, tiled=True),
        0,
        [],
    )
    for a in arrays:
        gathered.append(lax.slice_in_dim(result, at, at + a.shape[along], axis=along))
        at += a.shape[along]
    return tuple(gathered)


def sent_together_2(arrays, axis, dim, along):
    both = jnp.concatenate(arrays, axis=along)
    result, at, gathered = (lax.all_gather(both, axis, axis=dim, tiled=True), 0, [])
    for a in arrays:
        gathered.append(lax.slice_in_dim(result, at, at + a.shape[along], axis=along))
        at += a.shape[along]
    return tuple(gathered)


def local(
    tokens, norm_gain, gate_weight, up_weight, down_weight, group_pick, expert_pick, route_weight
):
    scaled = norm_gain[None, :, None]
    gate_local = (scaled * gate_weight).astype(jnp.bfloat16)
    up_local = (scaled * up_weight).astype(jnp.bfloat16)
    down_local = down_weight.astype(jnp.bfloat16)
    experts, rows_dev, cols_dev = gate_local.shape
    relaid = sent_together((gate_local, up_local, down_local), "fs", 0, 1, 2)
    gate_new, up_new, down_new = sent_together_2((relaid[0], relaid[1], relaid[2]), "gr", 1, 0)
    tok_rows, model_width = tokens.shape
    as_float = tokens.astype(jnp.float32)
    normed = (
        as_float * lax.rsqrt(jnp.mean(as_float * as_float, axis=-1, keepdims=True) + EPS)
    ).astype(jnp.bfloat16)
    per_group = experts // GROUPS
    top_count = expert_pick.shape[1]
    capacity = top_count * tok_rows // experts
    flat_ids = (group_pick[:, None] * per_group + expert_pick).reshape(-1)
    onehot = (flat_ids[:, None] == jnp.arange(experts, dtype=jnp.int32)[None, :]).astype(jnp.int32)
    slot_index = jnp.sum(onehot * (jnp.cumsum(onehot, axis=0) - 1), axis=1)
    target = flat_ids * capacity + slot_index
    source = (
        jnp.zeros((experts * capacity,), jnp.int32)
        .at[target]
        .set(jnp.arange(top_count * tok_rows, dtype=jnp.int32) // top_count)
    )
    outgoing = normed[source].reshape(experts, capacity, model_width)
    share = capacity // lax.axis_size("tp")
    start = lax.axis_index("tp") * share
    my_share = lax.dynamic_slice_in_dim(outgoing, start, share, 1)
    landed = lax.all_to_all(my_share, "fs", split_axis=0, concat_axis=1, tiled=True).reshape(
        experts, share, model_width
    )
    arrived = lax.all_gather(landed, "tp", axis=1, tiled=True).reshape(-1, model_width)
    gate_acts = jnp.dot(arrived, gate_new[0], preferred_element_type=jnp.float32)
    up_acts = jnp.dot(arrived, up_new[0], preferred_element_type=jnp.float32)
    hidden = (jax.nn.silu(gate_acts) * up_acts).astype(jnp.bfloat16)
    partial_value = lax.dot_general(
        hidden, down_new[0], (((1,), (1,)), ((), ())), preferred_element_type=jnp.float32
    ).astype(jnp.bfloat16)
    summed = (
        lax.psum_scatter(partial_value, "tp", scatter_dimension=1, tiled=True)
        .astype(jnp.float32)
        .astype(jnp.bfloat16)
    )
    returned = lax.all_to_all(summed, "fs", split_axis=0, concat_axis=0, tiled=True)
    picked = returned[target].reshape(tok_rows, top_count, -1).astype(jnp.float32)
    combined = jnp.sum(route_weight[:, :, None] * picked, axis=1).astype(jnp.bfloat16)
    return (combined, gate_new, up_new, down_new)


def solution(mesh):
    in_specs = (
        P(("gr", "fs"), None),
        P(("gr", "fs")),
        P(None, ("gr", "fs"), "tp"),
        P(None, ("gr", "fs"), "tp"),
        P(None, ("gr", "fs"), "tp"),
        P(("gr", "fs")),
        P(("gr", "fs"), None),
        P(("gr", "fs"), None),
    )
    out_specs = (
        P(("gr", "fs"), "tp"),
        P("fs", None, "tp"),
        P("fs", None, "tp"),
        P("fs", None, "tp"),
    )
    return jax.shard_map(local, mesh=mesh, in_specs=in_specs, out_specs=out_specs, check_vma=False)
```

profile of v0, /device:TPU:1, one launch (start us, length us, event | category | flops | bytes accessed | tf_op | source)
XLA Modules:
  0.0 474.9 jit_solution(10006823259516421929)
XLA Ops:
  7.2 1.9 convert_element_type.42
  9.5 2.1 multiply_convert_fusion.2
  11.7 1.9 pad_maximum_fusion
  13.6 9.3 %all-to-all-start.1 = ((bf16[32,48,1152]{2,1,0:T(8,128)(2,1)}), bf16[32,48,1152]{2,1,0:T(8,128)(2,1)S(1)}, u32[]{:S(2)}, u32[]{:S(2)}) async-start(bf16[32,48,1152]{2,1,0:T(8,128)(2,1)} %pad_maximum_fusion), calls=%async_computation.1 | async-start | bytes 7077888 | tf_op jit(solution)/shard_map/all_to_all | solution.py:15
  23.6 1.0 copy.15
  24.7 1.3 eq.29
  26.0 1.9 eq.25
  28.6 17.7 %reduce-window.6 = s32[32,16,128]{2,1,0:T(8,128)} reduce-window(s32[32,16,128]{2,1,0:T(8,128)} %fusion.10, s32[]{:T(128)} %constant.39.clone.1), window={size=1x1x128 pad=0_0x0_0x127_0}, to_apply=%region_1.0 | reduce-window | flops 8323072 | bytes 524292 | tf_op jit(solution)/shard_map/reduce-window
  46.3 1.8 slice.36
  48.1 1.8 copy.19
  49.9 0.9 reduce-window.9
  50.8 1.7 copy.14
  52.5 2.0 mul.77
  54.4 1.1 add_add_fusion
  56.3 4.1 fusion
  60.4 7.8 %fusion.1 = bf16[1024,3072]{1,0:T(8,128)(2,1)} fusion(bf16[1024,3072]{1,0:T(8,128)(2,1)} %param.8, f32[1024]{0:T(1024)S(1)} %add_rsqrt_fusion), kind=kLoop, calls=%fused_computation.6 | loop fusion | flops 9437184 | bytes 12587008 | tf_op jit(solution)/shard_map/convert_element_type | solution.py:48
  68.5 2.0 pad_maximum_fusion.1
  71.3 8.0 %scatter_custom_fusion = s32[2048]{0:T(1024)S(1)} fusion(s32[2048]{0:T(1024)S(1)} %bitcast.42, s32[2048]{0:T(1024)S(1)} %add_select_fusion, s32[]{:T(128)} %constant.39.clone.1), kind=kCustom, calls=%fused_computation.39 | custom fusion | bytes 8196 | tf_op jit(solution)/shard_map/scatter | solution.py:59
  79.4 26.7 %gather_fusion = bf16[2048,3072]{1,0:T(8,128)(2,1)} fusion(bf16[1024,3072]{1,0:T(8,128)(2,1)} %fusion.1, s32[2048]{0:T(1024)S(1)} %fusion.13), kind=kCustom, calls=%fused_computation | custom fusion | bytes 25174016 | tf_op jit(solution)/shard_map/gather | solution.py:61
  106.1 3.2 constant_dynamic-slice_fusion
  109.3 81.6 %all_to_all.33 = bf16[32,32,3072]{2,1,0:T(8,128)(2,1)} all-to-all(bf16[32,32,3072]{2,1,0:T(8,128)(2,1)S(1)} %constant_dynamic-slice_fusion), channel_id=1, replica_groups=mesh['gr'=2,'fs'=32,'tp'=2] {'fs'}, dimensions={0} | all-to-all | bytes 12582912 | tf_op jit(solution)/shard_map/all_to_all | solution.py:65
  191.2 42.5 %all-gather.5.cloned.1.call-done = bf16[3,3072,384]{2,1,0:T(8,128)(2,1)} async-done(((bf16[3,1536,384]{2,1,0:T(8,128)(2,1)}), bf16[3,3072,384]{2,1,0:T(8,128)(2,1)}) %all-gather.5.cloned.1.call-update) | async-done | bytes 7077904 | tf_op jit(solution)/shard_map/all_gather | solution.py:27
  233.7 6.0 %fusion.18 = (bf16[1,3072,384]{2,1,0:T(8,128)(2,1)S(1)}, bf16[1,3072,384]{2,1,0:T(8,128)(2,1)}, bf16[1,3072,384]{2,1,0:T(8,128)(2,1)}) fusion(bf16[3,3072,384]{2,1,0:T(8,128)(2,1)} %all-gather.5.cloned.1.call-done), kind=kLoop, calls=%fused_computation.45 | loop fusion | bytes 14155776 | tf_op jit(solution)/shard_map/slice | solution.py:29
  239.7 22.8 %all-gather.3.cloned.1.call-done = bf16[32,64,3072]{2,1,0:T(8,128)(2,1)} async-done(((bf16[32,32,3072]{2,1,0:T(8,128)(2,1)}), bf16[32,64,3072]{2,1,0:T(8,128)(2,1)}) %all-gather.3.cloned.1.call-update) | async-done | bytes 12582928 | tf_op jit(solution)/shard_map/all_gather | solution.py:68
  262.5 11.4 %fusion.5 = f32[2048,384]{1,0:T(8,128)} fusion(bf16[2048,3072]{1,0:T(8,128)(2,1)} %bitcast.44, bf16[1,3072,384]{2,1,0:T(8,128)(2,1)} %get-tuple-element.8), kind=kOutput, calls=%fused_computation.14 | convolution fusion | flops 4831838208 | bytes 18087936 | tf_op jit(solution)/shard_map/dot_general | solution.py:69
  274.0 19.9 %convolution_convert_fusion = bf16[2048,3072]{1,0:T(8,128)(2,1)} fusion(bf16[1,3072,384]{2,1,0:T(8,128)(2,1)} %get-tuple-element.7, f32[2048,384]{1,0:T(8,128)} %fusion.5, bf16[2048,3072]{1,0:T(8,128)(2,1)} %bitcast.45, bf16[1,3072,384]{2,1,0:T(8,128)(2,1)S(1)} %get-tuple-element.6), kind=kOutput, calls=%fused_computation.8 | convolution fusion | flops 9674686464 | bytes 33030144 | tf_op jit(solution)/shard_map/dot_general | solution.py:72
  293.9 23.5 %reduce-scatter.2.cloned.1.call-done = bf16[2048,1536]{1,0:T(8,128)(2,1)} async-done(((bf16[2048,3072]{1,0:T(8,128)(2,1)}), bf16[2048,1536]{1,0:T(8,128)(2,1)}) %reduce-scatter.2.cloned.1.call-update) | async-done | bytes 6291472 | tf_op jit(solution)/shard_map/reduce_scatter | solution.py:76
  317.4 8.5 %all-to-all-start.2 = ((bf16[32,64,1536]{2,1,0:T(8,128)(2,1)}), bf16[32,64,1536]{2,1,0:T(8,128)(2,1)}, u32[]{:S(2)}, u32[]{:S(2)}) async-start(bf16[32,64,1536]{2,1,0:T(8,128)(2,1)} %bitcast.37), calls=%async_computation.3 | async-start | bytes 12582912 | tf_op jit(solution)/shard_map/all_to_all | solution.py:80
  326.1 88.8 %all-to-all-done.2 = bf16[32,64,1536]{2,1,0:T(8,128)(2,1)} async-done(((bf16[32,64,1536]{2,1,0:T(8,128)(2,1)}), bf16[32,64,1536]{2,1,0:T(8,128)(2,1)}, u32[]{:S(2)}, u32[]{:S(2)}) %all-to-all-start.2) | async-done | bytes 6291488 | tf_op jit(solution)/shard_map/all_to_all | solution.py:80
  414.9 16.9 %gather_fusion.1 = bf16[2048,1536]{1,0:T(8,128)(2,1)} fusion(bf16[2048,1536]{1,0:T(8,128)(2,1)} %bitcast.12, s32[2048]{0:T(1024)S(1)} %broadcast_clamp_fusion), kind=kCustom, calls=%fused_computation.1 | custom fusion | bytes 12591104 | tf_op jit(solution)/shard_map/gather | solution.py:81
  431.8 14.1 %reshape.90 = f32[1024,2,1536]{2,1,0:T(2,128)} reshape(bf16[2048,1536]{1,0:T(8,128)(2,1)} %gather_fusion.1) | data formatting | bytes 18874368 | tf_op jit(solution)/shard_map/convert_element_type | solution.py:81
  445.9 22.4 %multiply_reduce_fusion = bf16[1024,1536]{1,0:T(8,128)(2,1)} fusion(f32[1024,2,1536]{2,1,0:T(2,128)} %reshape.90, f32[1024,2]{1,0:T(8,128)S(1)} %copy.13), kind=kLoop, calls=%fused_computation.7 | loop fusion | flops 4718592 | bytes 15736832 | tf_op jit(solution)/shard_map/reduce_sum | solution.py:82
  (32 shorter events, 4.2 us)
Async XLA Ops:
  7.2 2.4 copy-start
  7.2 2.4 copy-start.6
  13.6 9.4 %copy-start.5 = (s32[1024]{0:T(1024)S(1)}, s32[1024]{0:T(1024)}, u32[]{:S(2)}) copy-start(s32[1024]{0:T(1024)} %param.13) | copy-start | bytes 12292
  13.6 9.4 %copy-start.4 = (s32[1024,2]{0,1:T(2,128)S(1)}, s32[1024,2]{0,1:T(2,128)}, u32[]{:S(2)}) copy-start(s32[1024,2]{0,1:T(2,128)} %param.14) | copy-start | bytes 24580
  13.6 54.6 %all-to-all-start.1 = ((bf16[32,48,1152]{2,1,0:T(8,128)(2,1)}), bf16[32,48,1152]{2,1,0:T(8,128)(2,1)S(1)}, u32[]{:S(2)}, u32[]{:S(2)}) async-start(bf16[32,48,1152]{2,1,0:T(8,128)(2,1)} %pad_maximum_fusion), calls=%async_computation.1 | async-start | bytes 7077888 | tf_op jit(solution)/shard_map/all_to_all | solution.py:15
  22.9 210.8 %all-gather.5.cloned.1.call-start = ((), (), s32[]{:S(2)}) async-start(), calls=%async_computation.5 | async-start | bytes 10616832 | tf_op jit(solution)/shard_map/all_gather | solution.py:27
  70.6 0.7 copy-start.2
  70.6 191.9 %all-gather.3.cloned.1.call-start = ((), (), s32[]{:S(2)}) async-start(), calls=%async_computation.4 | async-start | bytes 18874368 | tf_op jit(solution)/shard_map/all_gather | solution.py:68
  191.0 126.4 %reduce-scatter.2.cloned.1.call-start = ((), (), s32[]{:S(2)}) async-start(), calls=%async_computation.6 | async-start | bytes 18874368 | tf_op jit(solution)/shard_map/reduce_scatter | solution.py:76
  239.7 34.3 %copy-start.1 = (bf16[1,3072,384]{2,1,0:T(8,128)(2,1)}, bf16[1,3072,384]{2,1,0:T(8,128)(2,1)S(1)}, u32[]{:S(2)}) copy-start(bf16[1,3072,384]{2,1,0:T(8,128)(2,1)S(1)} %get-tuple-element.6) | copy-start | bytes 7077892
  317.4 8.5 %copy-start.3 = (f32[1024,2]{0,1:T(2,128)S(1)}, f32[1024,2]{0,1:T(2,128)}, u32[]{:S(2)}) copy-start(f32[1024,2]{0,1:T(2,128)} %param.15) | copy-start | bytes 24580
  317.4 97.6 %all-to-all-start.2 = ((bf16[32,64,1536]{2,1,0:T(8,128)(2,1)}), bf16[32,64,1536]{2,1,0:T(8,128)(2,1)}, u32[]{:S(2)}, u32[]{:S(2)}) async-start(bf16[32,64,1536]{2,1,0:T(8,128)(2,1)} %bitcast.37), calls=%async_computation.3 | async-start | bytes 12582912 | tf_op jit(solution)/shard_map/all_to_all | solution.py:80
Sparse Core Ops, SparseCore 0:
  70.7 162.9 all-gather.4
  235.4 27.0 all-gather.2
  294.0 23.2 reduce-scatter.1
where the time goes:
time: 477 us; the launch traced here: 475 us
  waiting for transfers between devices  178 us (37%)
  local copies, waits for them, and re-layouts  88.1 us (18%)
  blocking collectives  81.6 us (17%)
  other arithmetic  64.1 us (13%)
  matrix products  31.4 us (7%)
  starting transfers between devices  18.1 us (4%)
  between operations  13.9 us (3%)
    all_to_all x1, waiting for transfers between devices, local(): lax.all_to_all(summed, 'fs', split_axis=0, concat_axis=0, tiled=True)  88.8 us
    all_to_all x1, blocking collectives, local(): lax.all_to_all(my_share, 'fs', split_axis=0, concat_axis=1, tiled=True)  81.6 us
    all_gather x1, waiting for transfers between devices, sent_together_2(): lax.all_gather(both, axis, axis=dim, tiled=True)  42.5 us
    gather x1, local copies, waits for them, and re-layouts, local(): outgoing = normed[source].reshape(experts, capacity, model_width)  26.7 us
    reduce_scatter x1, waiting for transfers between devices, local(): lax.psum_scatter(partial_value, 'tp', scatter_dimension=1, tiled=True)  23.5 us
    all_gather x1, waiting for transfers between devices, local(): lax.all_gather(landed, 'tp', axis=1, tiled=True).reshape(-1, model_width)  22.8 us
    reduce_sum x1, other arithmetic, local(): jnp.sum(route_weight[:, :, None] * picked, axis=1).astype(jnp.bfloat16)  22.4 us
    dot_general x1, matrix products, local(): lax.dot_general(hidden, down_new[0], (((1,), (1,)), ((), ())), preferred_...  19.9 us
  transfers between devices with their start and end apart: 5, of which 4 were waited for; matrix products, arithmetic and copies ran while one was open for 19% of the time, Pallas kernels for 0%

commit v1 on v0

v1 whole, which is shorter than its diff:
```python
import functools

import jax
import jax.numpy as jnp
from jax import lax
from jax.experimental import pallas as pl
from jax.experimental.pallas import tpu as pltpu
from jax.sharding import PartitionSpec as P

GROUPS = 4
EPS = 1e-06
BF = jnp.bfloat16
F32 = jnp.float32


def sent_together(arrays, axis, split_dim, concat_dim, along):
    both = jnp.concatenate(arrays, axis=along)
    result, at, gathered = (
        lax.all_to_all(both, axis, split_axis=split_dim, concat_axis=concat_dim, tiled=True),
        0,
        [],
    )
    for a in arrays:
        gathered.append(lax.slice_in_dim(result, at, at + a.shape[along], axis=along))
        at += a.shape[along]
    return tuple(gathered)


def sent_together_2(arrays, axis, dim, along):
    both = jnp.concatenate(arrays, axis=along)
    result, at, gathered = (lax.all_gather(both, axis, axis=dim, tiled=True), 0, [])
    for a in arrays:
        gathered.append(lax.slice_in_dim(result, at, at + a.shape[along], axis=along))
        at += a.shape[along]
    return tuple(gathered)


def dispatch_kernel(experts, share, ids_ref, tok_ref, out_ref, tgt_ref, select, normed):
    rows = tok_ref.shape[0]
    width = out_ref.shape[1]
    step = pl.program_id(0)

    @pl.when(step == 0)
    def _():
        first = lax.axis_index("tp") * share
        ids0, ids1 = ids_ref[0:1, :], ids_ref[1:2, :]
        which = lax.broadcasted_iota(jnp.int32, (experts, rows), 0)
        named0, named1 = ids0 == which, ids1 == which
        named = named0 | named1
        before = (
            lax.broadcasted_iota(jnp.int32, (rows, rows), 0)
            < lax.broadcasted_iota(jnp.int32, (rows, rows), 1)
        )
        rank = jnp.dot(
            jnp.where(named, 1.0, 0.0).astype(BF),
            jnp.where(before, 1.0, 0.0).astype(BF),
            preferred_element_type=F32,
        )
        capacity = 2 * share
        rank0 = jnp.sum(jnp.where(named0, rank, 0.0), axis=0, keepdims=True)
        rank1 = jnp.sum(jnp.where(named1, rank, 0.0), axis=0, keepdims=True)
        tgt_ref[0:1, :] = ids0 * capacity + rank0.astype(jnp.int32)
        tgt_ref[1:2, :] = ids1 * capacity + rank1.astype(jnp.int32)
        own = jnp.where(named, rank, -1.0).astype(jnp.int32)
        slot = lax.broadcasted_iota(jnp.int32, (share, rows), 0) + first
        for e in range(experts):
            hit = own[e : e + 1, :] == slot
            select[e * share : (e + 1) * share, :] = jnp.where(hit, 1.0, 0.0).astype(BF)

        @pl.loop(0, rows // 64)
        def _(r):
            at = pl.ds(pl.multiple_of(r * 64, 64), 64)
            x = tok_ref[at, :].astype(F32)
            scale = lax.rsqrt(jnp.mean(x * x, axis=-1, keepdims=True) + EPS)
            normed[at, :] = (x * scale).astype(BF)

    cols = pl.ds(pl.multiple_of(step * width, width), width)
    out_ref[...] = jnp.dot(select[...], normed[:, cols], preferred_element_type=F32).astype(BF)


def dispatch(ids, tokens, experts, share):
    rows, width = tokens.shape
    block = 512
    return pl.pallas_call(
        functools.partial(dispatch_kernel, experts, share),
        grid=(width // block,),
        out_shape=(
            jax.ShapeDtypeStruct((experts * share, width), BF),
            jax.ShapeDtypeStruct((2, rows), jnp.int32),
        ),
        in_specs=[
            pl.BlockSpec((2, rows), lambda i: (0, 0)),
            pl.BlockSpec((rows, width), lambda i: (0, 0)),
        ],
        out_specs=(
            pl.BlockSpec((experts * share, block), lambda i: (0, i)),
            pl.BlockSpec((2, rows), lambda i: (0, 0)),
        ),
        scratch_shapes=[
            pltpu.VMEM((experts * share, rows), BF),
            pltpu.VMEM((rows, width), BF),
        ],
        compiler_params=pltpu.CompilerParams(vmem_limit_bytes=48 * 1024 * 1024),
        cost_estimate=pl.CostEstimate(
            flops=2 * experts * share * rows * width,
            bytes_accessed=4 * rows * width,
            transcendentals=0,
        ),
        name="dispatch",
    )(ids, tokens)


def combine_kernel(tgt_ref, w_ref, rows_ref, out_ref, mix):
    @pl.when(pl.program_id(0) == 0)
    def _():
        slots = mix.shape[1]
        tile = 128

        @pl.loop(0, mix.shape[0] // tile)
        def _(r):
            at = pl.ds(pl.multiple_of(r * tile, tile), tile)
            slot = lax.broadcasted_iota(jnp.int32, (tile, slots), 1)
            t, w = tgt_ref[at, :], w_ref[at, :]
            mix[at, :] = jnp.where(
                slot == t[:, 0:1], w[:, 0:1], jnp.where(slot == t[:, 1:2], w[:, 1:2], 0.0)
            ).astype(BF)

    out_ref[...] = jnp.dot(mix[...], rows_ref[...], preferred_element_type=F32).astype(BF)


def combine(targets, weights, returned):
    rows = targets.shape[0]
    slots, width = returned.shape
    block = 512
    return pl.pallas_call(
        combine_kernel,
        grid=(width // block,),
        out_shape=jax.ShapeDtypeStruct((rows, width), BF),
        in_specs=[
            pl.BlockSpec((rows, 2), lambda i: (0, 0)),
            pl.BlockSpec((rows, 2), lambda i: (0, 0)),
            pl.BlockSpec((slots, block), lambda i: (0, i)),
        ],
        out_specs=pl.BlockSpec((rows, block), lambda i: (0, i)),
        scratch_shapes=[pltpu.VMEM((rows, slots), BF)],
        compiler_params=pltpu.CompilerParams(vmem_limit_bytes=48 * 1024 * 1024),
        cost_estimate=pl.CostEstimate(
            flops=2 * rows * slots * width, bytes_accessed=4 * slots * width, transcendentals=0
        ),
        name="combine",
    )(targets, weights, returned)


def local(
    tokens, norm_gain, gate_weight, up_weight, down_weight, group_pick, expert_pick, route_weight
):
    scaled = norm_gain[None, :, None]
    gate_local = (scaled * gate_weight).astype(BF)
    up_local = (scaled * up_weight).astype(BF)
    down_local = down_weight.astype(BF)
    experts = gate_local.shape[0]
    relaid = sent_together((gate_local, up_local, down_local), "fs", 0, 1, 2)
    gate_new, up_new, down_new = sent_together_2((relaid[0], relaid[1], relaid[2]), "gr", 1, 0)
    tok_rows, model_width = tokens.shape
    per_group = experts // GROUPS
    top_count = expert_pick.shape[1]
    capacity = top_count * tok_rows // experts
    share = capacity // lax.axis_size("tp")
    ids = group_pick[None, :] * per_group + expert_pick.T
    my_share, targets = dispatch(ids, tokens, experts, share)
    landed = lax.all_to_all(
        my_share.reshape(experts, share, model_width), "fs", split_axis=0, concat_axis=1, tiled=True
    ).reshape(experts, share, model_width)
    arrived = lax.all_gather(landed, "tp", axis=1, tiled=True).reshape(-1, model_width)
    gate_acts = jnp.dot(arrived, gate_new[0], preferred_element_type=jnp.float32)
    up_acts = jnp.dot(arrived, up_new[0], preferred_element_type=jnp.float32)
    hidden = (jax.nn.silu(gate_acts) * up_acts).astype(BF)
    partial_value = lax.dot_general(
        hidden, down_new[0], (((1,), (1,)), ((), ())), preferred_element_type=jnp.float32
    ).astype(BF)
    summed = lax.psum_scatter(partial_value, "tp", scatter_dimension=1, tiled=True)
    returned = lax.all_to_all(summed, "fs", split_axis=0, concat_axis=0, tiled=True)
    combined = combine(targets.T, route_weight, returned)
    return (combined, gate_new, up_new, down_new)


def solution(mesh):
    in_specs = (
        P(("gr", "fs"), None),
        P(("gr", "fs")),
        P(None, ("gr", "fs"), "tp"),
        P(None, ("gr", "fs"), "tp"),
        P(None, ("gr", "fs"), "tp"),
        P(("gr", "fs")),
        P(("gr", "fs"), None),
        P(("gr", "fs"), None),
    )
    out_specs = (
        P(("gr", "fs"), "tp"),
        P("fs", None, "tp"),
        P("fs", None, "tp"),
        P("fs", None, "tp"),
    )
    return jax.shard_map(local, mesh=mesh, in_specs=in_specs, out_specs=out_specs, check_vma=False)
```

time: 477 us -> 428 us (0.90)
  local copies, waits for them, and re-layouts: 88.1 us -> 7.79 us
  other arithmetic: 64.1 us -> 6.63 us
  blocking collectives: 81.6 us -> 130 us
  Pallas kernels: 0 us -> 28.2 us
  waiting for transfers between devices: 178 us -> 201 us
  starting transfers between devices: 18.1 us -> 8.39 us
    all_to_all x1 -> x2, blocking collectives: 81.6 us -> 130 us  [the longest x1 78.8 us: local(): lax.all_to_all(my_share.reshape(experts, share, model_width), 'fs', split...]
    gather x2 -> x0, local copies, waits for them, and re-layouts: 43.6 us -> none  [the longest x1 26.7 us: local(): outgoing = normed[source].reshape(experts, capacity, model_width)]
    pallas_call x0 -> x2, Pallas kernels: none -> 28.2 us  [the longest x1 15.1 us: dispatch(): pl.pallas_call(functools.partial(dispatch_kernel, experts, share), grid=(...]
    reduce_sum x3 -> x0, other arithmetic: 27.3 us -> none  [the longest x1 22.4 us: local(): jnp.sum(route_weight[:, :, None] * picked, axis=1).astype(jnp.bfloat16)]
    all_gather x1, waiting for transfers between devices: 42.5 us -> 66.9 us  [sent_together_2(): lax.all_gather(both, axis, axis=dim, tiled=True)]
    another operation x2 -> x0, other arithmetic: 18.6 us -> none
    convert_element_type x1 -> x0, local copies, waits for them, and re-layouts: 14.1 us -> none  [local(): returned[target].reshape(tok_rows, top_count, -1).astype(jnp.float32)]
    all_to_all x1 -> x0, starting transfers between devices: 9.34 us -> none  [sent_together(): lax.all_to_all(both, axis, split_axis=split_dim, concat_axis=concat_dim,...]
  transfers between devices with their start and end apart: 5 -> 4, of which waited for: 4 -> 4; matrix products, arithmetic and copies ran while one was open for 19% -> 2% of each run, Pallas kernels for 0% -> 4%
where the time goes in v1:
time: 428 us; the launch traced here: 427 us
  waiting for transfers between devices  201 us (47%)
  blocking collectives  130 us (30%)
  matrix products  31.4 us (7%)
  Pallas kernels  28.2 us (7%)
  between operations  13.8 us (3%)
  starting transfers between devices  8.39 us (2%)
  local copies, waits for them, and re-layouts  7.79 us (2%)
  other arithmetic  6.63 us (2%)
    all_to_all x1, waiting for transfers between devices, local(): lax.all_to_all(summed, 'fs', split_axis=0, concat_axis=0, tiled=True)  87.6 us
    all_to_all x1, blocking collectives, local(): lax.all_to_all(my_share.reshape(experts, share, model_width), 'fs', split...  78.8 us
    all_gather x1, waiting for transfers between devices, sent_together_2(): lax.all_gather(both, axis, axis=dim, tiled=True)  66.9 us
    all_to_all x1, blocking collectives, sent_together(): lax.all_to_all(both, axis, split_axis=split_dim, concat_axis=concat_dim,...  51.2 us
    reduce_scatter x1, waiting for transfers between devices, local(): lax.psum_scatter(partial_value, 'tp', scatter_dimension=1, tiled=True)  23.5 us
    all_gather x1, waiting for transfers between devices, local(): lax.all_gather(landed, 'tp', axis=1, tiled=True).reshape(-1, model_width)  22.8 us
    dot_general x1, matrix products, local(): lax.dot_general(hidden, down_new[0], (((1,), (1,)), ((), ())), preferred_...  20 us
    pallas_call x1, Pallas kernels, dispatch(): pl.pallas_call(functools.partial(dispatch_kernel, experts, share), grid=(...  15.1 us
  transfers between devices with their start and end apart: 4, of which 4 were waited for; matrix products, arithmetic and copies ran while one was open for 2% of the time, Pallas kernels for 4%

profile of v1, /device:TPU:1, one launch (start us, length us, event | category | flops | bytes accessed | tf_op | source)
XLA Modules:
  0.0 427.0 jit_solution(17886701053794535123)
XLA Ops:
  7.2 0.0 copy-start
  7.2 0.0 copy-start.5
  7.2 0.0 all-gather.5.cloned.1.call-start
  7.2 1.9 convert_element_type.17
  9.2 0.4 copy-done
  9.5 0.0 copy-done.5
  9.5 2.3 multiply_convert_fusion.2
  11.8 0.4 pad_maximum_fusion
  12.2 51.2 %all_to_all.32 = bf16[32,48,1152]{2,1,0:T(8,128)(2,1)S(1)} all-to-all(bf16[32,48,1152]{2,1,0:T(8,128)(2,1)S(1)} %pad_maximum_fusion), channel_id=1, replica_groups=mesh['gr'=2,'fs'=32,'tp'=2] {'fs'}, dimensions={0} | all-to-all | bytes 7077888 | tf_op jit(solution)/shard_map/all_to_all | solution.py:19
  63.4 0.4 fusion.8
  63.7 2.0 pad_maximum_fusion.1
  65.8 0.0 all-gather.5.cloned.1.call-update
  65.8 0.0 all-gather.3.cloned.1.call-start
  65.8 0.6 copy-done.4
  66.5 0.0 copy-done.3
  66.5 15.1 %dispatch.1 = (bf16[1024,3072]{1,0:T(8,128)(2,1)}, s32[2,1024]{1,0:T(2,128)S(1)}) custom-call(s32[2,1024]{1,0:T(2,128)S(1)} %add_bitcast_fusion.ids_ref, bf16[1024,3072]{1,0:T(8,128)(2,1)} %tok_ref.1), custom_call_target="tpu_custom_call" | custom-call | flops 6442450944 | bytes 12582912 | tf_op jit(solution)/shard_map/dispatch/pallas_call | solution.py:84
  81.6 78.8 %all_to_all.33 = bf16[32,32,3072]{2,1,0:T(8,128)(2,1)} all-to-all(bf16[32,32,3072]{2,1,0:T(8,128)(2,1)} %bitcast.23), channel_id=1, replica_groups=mesh['gr'=2,'fs'=32,'tp'=2] {'fs'}, dimensions={0} | all-to-all | bytes 12582912 | tf_op jit(solution)/shard_map/all_to_all | solution.py:171
  160.4 0.0 all-gather.3.cloned.1.call-update
  160.4 0.0 reduce-scatter.2.cloned.1.call-start
  160.5 66.9 %all-gather.5.cloned.1.call-done = bf16[3,3072,384]{2,1,0:T(8,128)(2,1)} async-done(((bf16[3,1536,384]{2,1,0:T(8,128)(2,1)}), bf16[3,3072,384]{2,1,0:T(8,128)(2,1)}) %all-gather.5.cloned.1.call-update) | async-done | bytes 7077904 | tf_op jit(solution)/shard_map/all_gather | solution.py:31
  227.4 6.0 %fusion.7 = (bf16[1,3072,384]{2,1,0:T(8,128)(2,1)S(1)}, bf16[1,3072,384]{2,1,0:T(8,128)(2,1)}, bf16[1,3072,384]{2,1,0:T(8,128)(2,1)}) fusion(bf16[3,3072,384]{2,1,0:T(8,128)(2,1)} %all-gather.5.cloned.1.call-done), kind=kLoop, calls=%fused_computation.14 | loop fusion | bytes 14155776 | tf_op jit(solution)/shard_map/slice | solution.py:33
  233.4 22.8 %all-gather.3.cloned.1.call-done = bf16[32,64,3072]{2,1,0:T(8,128)(2,1)} async-done(((bf16[32,32,3072]{2,1,0:T(8,128)(2,1)}), bf16[32,64,3072]{2,1,0:T(8,128)(2,1)}) %all-gather.3.cloned.1.call-update) | async-done | bytes 12582928 | tf_op jit(solution)/shard_map/all_gather | solution.py:174
  256.2 11.4 %fusion.3 = f32[2048,384]{1,0:T(8,128)} fusion(bf16[2048,3072]{1,0:T(8,128)(2,1)} %bitcast.24, bf16[1,3072,384]{2,1,0:T(8,128)(2,1)} %get-tuple-element.10), kind=kOutput, calls=%fused_computation.6 | convolution fusion | flops 4831838208 | bytes 18087936 | tf_op jit(solution)/shard_map/dot_general | solution.py:175
  267.6 0.0 copy-done.1
  267.6 20.0 %convolution_convert_fusion = bf16[2048,3072]{1,0:T(8,128)(2,1)} fusion(bf16[1,3072,384]{2,1,0:T(8,128)(2,1)} %get-tuple-element.9, f32[2048,384]{1,0:T(8,128)} %fusion.3, bf16[2048,3072]{1,0:T(8,128)(2,1)} %bitcast.25, bf16[1,3072,384]{2,1,0:T(8,128)(2,1)S(1)} %get-tuple-element.8), kind=kOutput, calls=%fused_computation | convolution fusion | flops 9674686464 | bytes 33030144 | tf_op jit(solution)/shard_map/dot_general | solution.py:178
  287.6 0.0 reduce-scatter.2.cloned.1.call-update
  287.6 23.5 %reduce-scatter.2.cloned.1.call-done = bf16[2048,1536]{1,0:T(8,128)(2,1)} async-done(((bf16[2048,3072]{1,0:T(8,128)(2,1)}), bf16[2048,1536]{1,0:T(8,128)(2,1)}) %reduce-scatter.2.cloned.1.call-update) | async-done | bytes 6291472 | tf_op jit(solution)/shard_map/reduce_scatter | solution.py:181
  311.1 8.3 %all-to-all-start.2 = ((bf16[32,64,1536]{2,1,0:T(8,128)(2,1)}), bf16[32,64,1536]{2,1,0:T(8,128)(2,1)}, u32[]{:S(2)}, u32[]{:S(2)}) async-start(bf16[32,64,1536]{2,1,0:T(8,128)(2,1)} %bitcast.22), calls=%async_computation.3 | async-start | bytes 12582912 | tf_op jit(solution)/shard_map/all_to_all | solution.py:182
  319.4 0.2 copy.12
  319.6 0.2 copy.13.w_ref
  319.8 87.6 %all-to-all-done.2 = bf16[32,64,1536]{2,1,0:T(8,128)(2,1)} async-done(((bf16[32,64,1536]{2,1,0:T(8,128)(2,1)}), bf16[32,64,1536]{2,1,0:T(8,128)(2,1)}, u32[]{:S(2)}, u32[]{:S(2)}) %all-to-all-start.2) | async-done | bytes 6291488 | tf_op jit(solution)/shard_map/all_to_all | solution.py:182
  407.4 13.1 %combine.1 = bf16[1024,1536]{1,0:T(8,128)(2,1)} custom-call(s32[1024,2]{1,0:T(8,128)S(1)} %bitcast.20, f32[1024,2]{1,0:T(8,128)S(1)} %copy.13.w_ref, bf16[2048,1536]{1,0:T(8,128)(2,1)} %bitcast.9.rows_ref), custom_call_target="tpu_custom_call" | custom-call | flops 6442450944 | bytes 12582912 | tf_op jit(solution)/shard_map/combine/pallas_call | solution.py:135
  (7 shorter events, 0.0 us)
Async XLA Ops:
  7.2 2.4 copy-start
  7.2 2.4 copy-start.5
  7.2 220.2 %all-gather.5.cloned.1.call-start = ((), (), s32[]{:S(2)}) async-start(), calls=%async_computation.5 | async-start | bytes 10616832 | tf_op jit(solution)/shard_map/all_gather | solution.py:31
  65.8 0.7 copy-start.4
  65.8 0.7 copy-start.3
  65.8 190.4 %all-gather.3.cloned.1.call-start = ((), (), s32[]{:S(2)}) async-start(), calls=%async_computation.4 | async-start | bytes 18874368 | tf_op jit(solution)/shard_map/all_gather | solution.py:174
  160.4 150.7 %reduce-scatter.2.cloned.1.call-start = ((), (), s32[]{:S(2)}) async-start(), calls=%async_computation.6 | async-start | bytes 18874368 | tf_op jit(solution)/shard_map/reduce_scatter | solution.py:181
  233.4 34.3 %copy-start.1 = (bf16[1,3072,384]{2,1,0:T(8,128)(2,1)}, bf16[1,3072,384]{2,1,0:T(8,128)(2,1)S(1)}, u32[]{:S(2)}) copy-start(bf16[1,3072,384]{2,1,0:T(8,128)(2,1)S(1)} %get-tuple-element.8) | copy-start | bytes 7077892
  311.1 8.5 %copy-start.2 = (f32[1024,2]{0,1:T(2,128)S(1)}, f32[1024,2]{0,1:T(2,128)}, u32[]{:S(2)}) copy-start(f32[1024,2]{0,1:T(2,128)} %param.15) | copy-start | bytes 24580
  311.1 96.3 %all-to-all-start.2 = ((bf16[32,64,1536]{2,1,0:T(8,128)(2,1)}), bf16[32,64,1536]{2,1,0:T(8,128)(2,1)}, u32[]{:S(2)}, u32[]{:S(2)}) async-start(bf16[32,64,1536]{2,1,0:T(8,128)(2,1)} %bitcast.22), calls=%async_computation.3 | async-start | bytes 12582912 | tf_op jit(solution)/shard_map/all_to_all | solution.py:182
Sparse Core Ops, SparseCore 0:
  65.9 161.4 all-gather.4
  229.1 27.0 all-gather.2
  287.8 23.2 reduce-scatter.1

commit v2 on v1

v2 whole, which is shorter than its diff:
```python
import functools

import jax
import jax.numpy as jnp
from jax import lax
from jax.experimental import pallas as pl
from jax.experimental.pallas import tpu as pltpu
from jax.sharding import PartitionSpec as P

GROUPS = 4
EPS = 1e-06
BF = jnp.bfloat16
F32 = jnp.float32
MESH = pl.DeviceIdType.MESH
MIB = 1024 * 1024
DYS = (2, 1, 3, 0)


def place():
    fs = lax.axis_index("fs")
    fz, y, x = fs // 16, (fs // 4) % 4, fs % 4
    return lax.axis_index("gr") * 2 + fz, fz, y, x, lax.axis_index("tp")


def dispatch_kernel(experts, share, ids_ref, tok_ref, out_ref, tgt_ref, select, normed, own):
    rows = tok_ref.shape[0]
    width = out_ref.shape[1]
    step = pl.program_id(0)

    @pl.when(step == 0)
    def _():
        _, fz, y, x, core = place()
        ids0, ids1 = ids_ref[0:1, :], ids_ref[1:2, :]
        which = lax.broadcasted_iota(jnp.int32, (experts, rows), 0)
        named0, named1 = ids0 == which, ids1 == which
        named = named0 | named1
        before = (
            lax.broadcasted_iota(jnp.int32, (rows, rows), 0)
            < lax.broadcasted_iota(jnp.int32, (rows, rows), 1)
        )
        rank = jnp.dot(
            jnp.where(named, 1.0, 0.0).astype(BF),
            jnp.where(before, 1.0, 0.0).astype(BF),
            preferred_element_type=F32,
        )
        capacity = 2 * share

        def row_of(ids, named_k):
            at = jnp.sum(jnp.where(named_k, rank, 0.0), axis=0, keepdims=True).astype(jnp.int32)
            far = (ids >> 4) ^ fz
            dy = ((ids >> 2) - y) & 3
            dx = (ids - x) & 3
            slot = jnp.where(dy == 2, 0, jnp.where(dy == 1, 1, jnp.where(dy == 3, 2, 3)))
            return far * (experts // 2 * capacity) + (slot * 4 + dx) * capacity + at

        tgt_ref[0:1, :] = row_of(ids0, named0)
        tgt_ref[1:2, :] = row_of(ids1, named1)
        own[...] = jnp.where(named, rank, -1.0).astype(jnp.int32)
        line = lax.broadcasted_iota(jnp.int32, (share, rows), 0)
        half = share // 2
        slots = (line + core * share, line + jnp.where(line < half, 0, half) + core * half)
        for j, dy in enumerate(DYS):
            for dx in range(4):
                for dz in range(2):
                    e = ((fz + dz) % 2) * 16 + ((y + dy) % 4) * 4 + (x + dx) % 4
                    at = ((j * 4 + dx) * 2 + dz) * share
                    hit = own[pl.ds(e, 1), :] == slots[dz]
                    select[at : at + share, :] = jnp.where(hit, 1.0, 0.0).astype(BF)

        @pl.loop(0, rows // 64)
        def _(r):
            at = pl.ds(pl.multiple_of(r * 64, 64), 64)
            v = tok_ref[at, :].astype(F32)
            scale = lax.rsqrt(jnp.mean(v * v, axis=-1, keepdims=True) + EPS)
            normed[at, :] = (v * scale).astype(BF)

    cols = pl.ds(pl.multiple_of(step * width, width), width)
    out_ref[...] = jnp.dot(select[...], normed[:, cols], preferred_element_type=F32).astype(BF)


def dispatch(ids, tokens, experts, share):
    rows, width = tokens.shape
    block = 512
    return pl.pallas_call(
        functools.partial(dispatch_kernel, experts, share),
        grid=(width // block,),
        out_shape=(
            jax.ShapeDtypeStruct((experts * share, width), BF),
            jax.ShapeDtypeStruct((2, rows), jnp.int32),
        ),
        in_specs=[
            pl.BlockSpec((2, rows), lambda i: (0, 0)),
            pl.BlockSpec((rows, width), lambda i: (0, 0)),
        ],
        out_specs=(
            pl.BlockSpec((experts * share, block), lambda i: (0, i)),
            pl.BlockSpec((2, rows), lambda i: (0, 0)),
        ),
        scratch_shapes=[
            pltpu.VMEM((experts * share, rows), BF),
            pltpu.VMEM((rows, width), BF),
            pltpu.VMEM((experts, rows), jnp.int32),
        ],
        compiler_params=pltpu.CompilerParams(vmem_limit_bytes=48 * MIB),
        cost_estimate=pl.CostEstimate(
            flops=2 * experts * share * rows * width,
            bytes_accessed=4 * rows * width,
            transcendentals=0,
        ),
        name="dispatch",
    )(ids, tokens)


def combine_kernel(tgt_ref, w_ref, rows_ref, out_ref, mix):
    @pl.when(pl.program_id(0) == 0)
    def _():
        slots = mix.shape[1]
        tile = 128

        @pl.loop(0, mix.shape[0] // tile)
        def _(r):
            at = pl.ds(pl.multiple_of(r * tile, tile), tile)
            slot = lax.broadcasted_iota(jnp.int32, (tile, slots), 1)
            t, w = tgt_ref[at, :], w_ref[at, :]
            mix[at, :] = jnp.where(
                slot == t[:, 0:1], w[:, 0:1], jnp.where(slot == t[:, 1:2], w[:, 1:2], 0.0)
            ).astype(BF)

    out_ref[...] = jnp.dot(mix[...], rows_ref[...], preferred_element_type=F32).astype(BF)


def combine(targets, weights, returned):
    rows = targets.shape[0]
    slots, width = returned.shape
    block = 512
    return pl.pallas_call(
        combine_kernel,
        grid=(width // block,),
        out_shape=jax.ShapeDtypeStruct((rows, width), BF),
        in_specs=[
            pl.BlockSpec((rows, 2), lambda i: (0, 0)),
            pl.BlockSpec((rows, 2), lambda i: (0, 0)),
            pl.BlockSpec((slots, block), lambda i: (0, i)),
        ],
        out_specs=pl.BlockSpec((rows, block), lambda i: (0, i)),
        scratch_shapes=[pltpu.VMEM((rows, slots), BF)],
        compiler_params=pltpu.CompilerParams(vmem_limit_bytes=48 * MIB),
        cost_estimate=pl.CostEstimate(
            flops=2 * rows * slots * width, bytes_accessed=4 * slots * width, transcendentals=0
        ),
        name="combine",
    )(targets, weights, returned)


def exchange_kernel(
    ms, wg, wu, wd, ret, og, ou, od,
    wx, wy, wf, tx, ty, lha, lhb, ps, po, ra, rb, rz, rya, ryb, send, recv, here,
):
    z, fz, y, x, core = place()
    used = {"away": 0, "near": 0}
    sent, local_copies = [], []

    def device(dz=0, dy=0, dx=0, flip=False):
        at_z = (z + dz) % 4
        return {
            "gr": at_z // 2,
            "fs": (at_z % 2) * 16 + ((y + dy) % 4) * 4 + (x + dx) % 4,
            "tp": 1 - core if flip else core,
        }

    def remote(src, dst, **to):
        at = used["away"]
        used["away"] += 1
        c = pltpu.make_async_remote_copy(
            src_ref=src,
            dst_ref=dst,
            send_sem=send.at[at],
            recv_sem=recv.at[at],
            device_id=device(**to),
            device_id_type=MESH,
        )
        c.start()
        sent.append(c)
        return c

    def near(src, dst):
        at = used["near"]
        used["near"] += 1
        c = pltpu.make_async_copy(src, dst, here.at[at])
        c.start()
        return c

    barrier = pltpu.get_barrier_semaphore()
    peers = [{"flip": True}] + [{axis: d} for axis in ("dz", "dy", "dx") for d in (1, 2, 3)]
    for to in peers:
        pl.semaphore_signal(barrier, inc=1, device_id=device(**to), device_id_type=MESH)
    pl.semaphore_wait(barrier, len(peers))

    stacks = (wg, wu, wd)
    pieces = [(k, dz) for k in range(3) for dz in (1, 0)]
    wx_own, wx_in = [], []
    for p, (k, dz) in enumerate(pieces):
        ez = (fz + dz) % 2
        wx_own.append(near(stacks[k].at[ez, :, x], wx.at[p, x]))
        wx_in.append(
            [remote(stacks[k].at[ez, :, (x + dx) % 4], wx.at[p, x], dx=dx) for dx in (2, 1, 3)]
        )
    tx_own, tx_in = [], []
    for j in range(4):
        to = tx if j < 3 else ty
        tx_own.append(near(ms.at[j, 0], to.at[j, 0]))
        tx_in.append([remote(ms.at[j, dx], to.at[j, dx], dx=dx) for dx in (2, 1, 3)])

    wy_own, wy_in, wf_own, wf_in = [], [], [], []

    def weights_y(p):
        wx_own[p].wait()
        for c in wx_in[p]:
            c.wait_recv()
        wy_own.append(near(wx.at[p, :, y], wy.at[p, y]))
        wy_in.append(
            [remote(wx.at[p, :, (y + dy) % 4], wy.at[p, y], dy=dy) for dy in (2, 1, 3)]
        )

    def weights_z(p):
        k, dz = pieces[p]
        wy_own[p].wait()
        for c in wy_in[p]:
            c.wait_recv()
        if dz == 0:
            wf_own.append(near(wy.at[p], wf.at[k, z]))
        for d in (2,) if dz == 0 else (1, 3):
            wf_in.append(remote(wy.at[p], wf.at[k, z], dz=d))

    ty_in, a_own, a_in, bz_in, b_in = [], [], [], [], []

    def tokens_y(j):
        tx_own[j].wait()
        for c in tx_in[j]:
            c.wait_recv()
        ty_in.append(remote(tx.at[j], ty.at[j], dy=DYS[j]))

    def tokens_z(j):
        if j < 3:
            ty_in[j].wait_recv()
        else:
            tx_own[3].wait()
            for c in tx_in[3]:
                c.wait_recv()
        half = ty.shape[3] // 2
        bz_in.append(
            [
                remote(ty.at[j, :, 1, pl.ds(h * half, half)], lhb.at[j, h, :, core], dz=d)
                for h, d in ((0, 1), (1, 3))
            ]
        )
        a_in.append(remote(ty.at[j, :, 0], lha.at[j, :, core], flip=True))
        a_own.append(near(ty.at[j, :, 0], lha.at[j, :, core]))

    def tokens_b(j):
        for c in bz_in[j]:
            c.wait_recv()
        b_in.append(
            [remote(lhb.at[j, h, :, core], lhb.at[j, h, :, core], flip=True) for h in range(2)]
        )

    weights_y(0)
    for p in range(1, 6):
        weights_y(p)
        weights_z(p - 1)
    weights_z(5)
    tokens_y(0)
    tokens_y(1)
    tokens_z(0)
    tokens_y(2)
    for j in (1, 2, 3):
        tokens_z(j)

    for c in wf_own:
        c.wait()
    for c in wf_in:
        c.wait_recv()
    written = [near(wf.at[k], out) for k, out in enumerate((og, ou, od))]

    width = wf.shape[-1]
    depth = wf.shape[2] * wf.shape[3] * wf.shape[4]

    def expert(rows, i):
        v = rows.reshape(-1, rows.shape[-1])
        gate = jnp.dot(v, wf[0].reshape(4 * depth, width), preferred_element_type=F32)
        up = jnp.dot(v, wf[1].reshape(4 * depth, width), preferred_element_type=F32)
        hidden = (gate / (1.0 + jnp.exp(-gate)) * up).astype(BF)

        def part(at_z):
            return lax.dot_general(
                hidden,
                wf[2, at_z].reshape(depth, width),
                (((1,), (1,)), ((), ())),
                preferred_element_type=F32,
            ).astype(BF).reshape(ps.shape[1:-1] + (depth,))

        for s in range(2):
            ps[i % 2, :, :, :, s * depth : (s + 1) * depth] = part((1 - core) * 2 + s)
        c = remote(ps.at[i % 2], ra.at[i] if i < 4 else rb.at[i - 4], flip=True)
        for s in range(2):
            po[i % 2, :, :, :, s * depth : (s + 1) * depth] = part(core * 2 + s)
        return c

    parts = []
    ry_in, rz_in, out_in, out_own = {}, {}, [], []

    def along_x(rows_of, part, j):
        out_own.append(near(rows_of(0), ret.at[part, j, 0]))
        for dx in (2, 1, 3):
            out_in.append(remote(rows_of(dx), ret.at[part, j, dx], dx=4 - dx))

    def near_rows(ref, j):
        return lambda dx: ref.at[j, dx // 2, pl.ds((dx % 2) * 2, 2)]

    def far_rows(ref, j):
        return lambda dx: ref.at[j, :, dx]

    def finish(i):
        parts[i].wait_recv()
        ref, j = (ra, i) if i < 4 else (rb, i - 4)
        ref[j] = (ref[j].astype(F32) + po[i % 2].astype(F32)).astype(BF)
        if i >= 4:
            rz_in[j] = [remote(rb.at[j, h], rz.at[j, h], dz=d) for h, d in ((0, 3), (1, 1))]
        elif j < 3:
            ry_in[j] = remote(ra.at[j], rya.at[j], dy=4 - DYS[j])
        else:
            along_x(near_rows(ra, 3), 0, 3)

    def near_back(j):
        ry_in[j].wait_recv()
        along_x(near_rows(rya, j), 0, j)

    def far_back_y(j):
        for c in rz_in[j]:
            c.wait_recv()
        if j < 3:
            ry_in[4 + j] = remote(rz.at[j], ryb.at[j], dy=4 - DYS[j])
        else:
            along_x(far_rows(rz, 3), 1, 3)

    def far_back_x(j):
        ry_in[4 + j].wait_recv()
        along_x(far_rows(ryb, j), 1, j)

    for i in range(8):
        if i < 4:
            a_own[i].wait()
            a_in[i].wait_recv()
        else:
            for c in b_in[i - 4]:
                c.wait_recv()
        if i >= 2:
            parts[i - 2].wait_send()
        parts.append(expert(lha[i] if i < 4 else lhb[i - 4], i))
        if 3 <= i < 7:
            tokens_b(i - 3)
        if i >= 1:
            finish(i - 1)
        if 3 <= i < 6:
            near_back(i - 3)
    finish(7)
    far_back_y(0)
    far_back_y(1)
    far_back_x(0)
    far_back_y(2)
    far_back_y(3)
    far_back_x(1)
    far_back_x(2)
    for c in out_in:
        c.wait_recv()
    for c in out_own + written:
        c.wait()
    waited = [id(c) for c in parts[:6]]
    for c in sent:
        if id(c) not in waited:
            c.wait_send()


def exchange(mine, gate, up, down):
    share, model = mine.shape[-2:]
    rows, width = gate.shape[-2:]
    half = share // 2
    cols = model // 2
    hbm = pl.BlockSpec(memory_space=pl.ANY)
    served = jax.ShapeDtypeStruct((4, 4, 4, rows, width), BF)
    back = (2, 4, share, cols)
    return pl.pallas_call(
        exchange_kernel,
        out_shape=(jax.ShapeDtypeStruct((2, 4, 4, 2, share, cols), BF), served, served, served),
        in_specs=[hbm] * 4,
        out_specs=(hbm,) * 4,
        scratch_shapes=[
            pltpu.VMEM((6, 4, 4, rows, width), BF),
            pltpu.VMEM((6, 4, 4, rows, width), BF),
            pltpu.VMEM((3, 4, 4, 4, rows, width), BF),
            pltpu.VMEM((3, 4, 2, share, model), BF),
            pltpu.VMEM((4, 4, 2, share, model), BF),
            pltpu.VMEM((4, 4, 2, share, model), BF),
            pltpu.VMEM((4, 2, 4, 2, half, model), BF),
            pltpu.VMEM((2,) + back, BF),
            pltpu.VMEM((2,) + back, BF),
            pltpu.VMEM((4,) + back, BF),
            pltpu.VMEM((4,) + back, BF),
            pltpu.VMEM((4,) + back, BF),
            pltpu.VMEM((3,) + back, BF),
            pltpu.VMEM((3,) + back, BF),
            pltpu.SemaphoreType.DMA((128,)),
            pltpu.SemaphoreType.DMA((128,)),
            pltpu.SemaphoreType.DMA((48,)),
        ],
        compiler_params=pltpu.CompilerParams(
            collective_id=0, has_side_effects=True, vmem_limit_bytes=63 * MIB
        ),
        name="exchange",
    )(mine, gate, up, down)


def local(
    tokens, norm_gain, gate_weight, up_weight, down_weight, group_pick, expert_pick, route_weight
):
    experts, rows, width = gate_weight.shape
    scaled = norm_gain[None, :, None]
    split = (2, 4, 4, rows, width)
    gate = (scaled * gate_weight).astype(BF).reshape(split)
    up = (scaled * up_weight).astype(BF).reshape(split)
    down = down_weight.astype(BF).reshape(split)
    tok_rows, model_width = tokens.shape
    top_count = expert_pick.shape[1]
    capacity = top_count * tok_rows // experts
    share = capacity // 2
    ids = group_pick[None, :] * (experts // GROUPS) + expert_pick.T
    mine, targets = dispatch(ids, tokens, experts, share)
    returned, gate_new, up_new, down_new = exchange(
        mine.reshape(4, 4, 2, share, model_width), gate, up, down
    )
    combined = combine(
        targets.T, route_weight, returned.reshape(experts * capacity, model_width // 2)
    )
    whole = (1, model_width, width)
    return (combined, gate_new.reshape(whole), up_new.reshape(whole), down_new.reshape(whole))


def solution(mesh):
    in_specs = (
        P(("gr", "fs"), None),
        P(("gr", "fs")),
        P(None, ("gr", "fs"), "tp"),
        P(None, ("gr", "fs"), "tp"),
        P(None, ("gr", "fs"), "tp"),
        P(("gr", "fs")),
        P(("gr", "fs"), None),
        P(("gr", "fs"), None),
    )
    out_specs = (
        P(("gr", "fs"), "tp"),
        P("fs", None, "tp"),
        P("fs", None, "tp"),
        P("fs", None, "tp"),
    )
    return jax.shard_map(local, mesh=mesh, in_specs=in_specs, out_specs=out_specs, check_vma=False)
```

time: 428 us -> 290 us (0.68)
  Pallas kernels: 28.2 us -> 276 us
  waiting for transfers between devices: 201 us -> 0 us
  blocking collectives: 130 us -> 0 us
  matrix products: 31.4 us -> 0 us
  between operations: 13.8 us -> 0.7 us
  starting transfers between devices: 8.39 us -> 0 us
    pallas_call x0 -> x1, Pallas kernels: none -> 247 us  [exchange(): pl.pallas_call(exchange_kernel, out_shape=(jax.ShapeDtypeStruct((2, 4, 4,...]
    all_to_all x2 -> x0, blocking collectives: 130 us -> none  [the longest x1 78.8 us: local(): lax.all_to_all(my_share.reshape(experts, share, model_width), 'fs', split...]
    all_gather x2 -> x0, waiting for transfers between devices: 89.8 us -> none  [the longest x1 66.9 us: sent_together_2(): lax.all_gather(both, axis, axis=dim, tiled=True)]
    all_to_all x1 -> x0, waiting for transfers between devices: 87.6 us -> none  [local(): lax.all_to_all(summed, 'fs', split_axis=0, concat_axis=0, tiled=True)]
    dot_general x2 -> x0, matrix products: 31.4 us -> none  [the longest x1 20 us: local(): lax.dot_general(hidden, down_new[0], (((1,), (1,)), ((), ())), preferred_...]
    reduce_scatter x1 -> x0, waiting for transfers between devices: 23.5 us -> none  [local(): lax.psum_scatter(partial_value, 'tp', scatter_dimension=1, tiled=True)]
    all_to_all x1 -> x0, starting transfers between devices: 8.27 us -> none  [local(): lax.all_to_all(summed, 'fs', split_axis=0, concat_axis=0, tiled=True)]
    slice x2 -> x0, local copies, waits for them, and re-layouts: 6.34 us -> none  [the longest x1 5.98 us: sent_together_2(): lax.slice_in_dim(result, at, at + a.shape[along], axis=along)]
  transfers between devices with their start and end apart: 4 -> 0, of which waited for: 4 -> 0; matrix products, arithmetic and copies ran while one was open for 2% -> 0% of each run, Pallas kernels for 4% -> 0%
where the time goes in v2:
time: 290 us; the launch traced here: 288 us
  Pallas kernels  276 us (95%)
  local copies, waits for them, and re-layouts  7.17 us (2%)
  other arithmetic  4.42 us (2%)
    pallas_call x1, Pallas kernels, exchange(): pl.pallas_call(exchange_kernel, out_shape=(jax.ShapeDtypeStruct((2, 4, 4,...  247 us
    pallas_call x1, Pallas kernels, dispatch(): pl.pallas_call(functools.partial(dispatch_kernel, experts, share), grid=(...  15.3 us
    pallas_call x1, Pallas kernels, combine(): pl.pallas_call(combine_kernel, grid=(width // block,), out_shape=jax.Shap...  13.2 us
    unnamed x20, local copies, waits for them, and re-layouts  6.95 us

profile of v2, /device:TPU:1, one launch (start us, length us, event | category | flops | bytes accessed | tf_op | source)
XLA Modules:
  0.0 288.3 jit_solution(9452050866579850957)
XLA Ops:
  0.6 0.7 broadcast_multiply_fusion
  1.3 0.7 add_bitcast_fusion.ids_ref
  2.0 0.0 copy-start
  2.0 0.0 copy-start.1
  2.0 0.0 copy-start.7
  2.0 15.3 %dispatch.1 = (bf16[1024,3072]{1,0:T(8,128)(2,1)}, s32[2,1024]{1,0:T(2,128)S(1)}) custom-call(s32[2,1024]{1,0:T(2,128)S(1)} %add_bitcast_fusion.ids_ref, bf16[1024,3072]{1,0:T(8,128)(2,1)} %tok_ref.1), custom_call_target="tpu_custom_call" | custom-call | flops 6442450944 | bytes 12582912 | tf_op jit(solution)/shard_map/dispatch/pallas_call | solution.py:84
  17.3 0.0 copy-done
  17.3 0.0 copy-done.1
  17.3 0.0 copy-done.7
  17.3 0.0 copy-start.2
  17.3 1.9 multiply_convert_fusion
  19.2 0.3 copy-done.2
  19.5 1.1 convert_element_type.11
  20.6 0.0 copy-start.6
  20.6 247.5 %exchange.1 = (bf16[2,4,4,2,32,1536]{5,4,3,2,1,0:T(8,128)(2,1)}, bf16[4,4,4,48,384]{4,3,2,1,0:T(8,128)(2,1)}, bf16[4,4,4,48,384]{4,3,2,1,0:T(8,128)(2,1)}, bf16[4,4,4,48,384]{4,3,2,1,0:T(8,128)(2,1)}) custom-call(bf16[4,4,2,32,3072]{4,3,2,1,0:T(8,128)(2,1)} %bitcast.12, bf16[2,4,4,48,384]{4,3,2,1,0:T(8,128)(2,1)} %bitcast.14, ...), custom_call_target="tpu_custom_call" | custom-call | tf_op jit(solution)/shard_map/exchange/pallas_call | solution.py:392
  268.1 0.2 copy.12
  268.4 0.0 copy-done.6
  268.4 0.2 copy.13.w_ref
  268.6 0.0 copy-start.5
  268.6 13.2 %combine.1 = bf16[1024,1536]{1,0:T(8,128)(2,1)} custom-call(s32[1024,2]{1,0:T(8,128)S(1)} %bitcast.11, f32[1024,2]{1,0:T(8,128)S(1)} %copy.13.w_ref, bf16[2048,1536]{1,0:T(8,128)(2,1)} %bitcast.19), custom_call_target="tpu_custom_call" | custom-call | flops 6442450944 | bytes 12582912 | tf_op jit(solution)/shard_map/combine/pallas_call | solution.py:136
  281.9 0.0 copy-done.5
  281.9 0.0 copy-start.4
  281.9 1.4 copy.17
  283.3 1.1 copy-done.4
  284.4 0.0 copy-start.3
  284.4 1.4 copy.18
  285.8 1.1 copy-done.3
  286.9 1.4 copy.19
Async XLA Ops:
  2.0 15.3 %copy-start = (f32[32,48,384]{2,1,0:T(8,128)S(1)}, f32[32,48,384]{2,1,0:T(8,128)}, u32[]{:S(2)}) copy-start(f32[32,48,384]{2,1,0:T(8,128)} %param.11) | copy-start | bytes 7077892
  2.0 15.3 %copy-start.1 = (f32[32,48,384]{2,1,0:T(8,128)S(1)}, f32[32,48,384]{2,1,0:T(8,128)}, u32[]{:S(2)}) copy-start(f32[32,48,384]{2,1,0:T(8,128)} %param.10) | copy-start | bytes 7077892
  2.0 15.3 %copy-start.7 = (f32[48]{0:T(128)S(1)}, f32[48]{0:T(128)}, u32[]{:S(2)}) copy-start(f32[48]{0:T(128)} %param.9) | copy-start | bytes 580
  17.3 2.2 copy-start.2
  20.6 247.7 %copy-start.6 = (f32[1024,2]{0,1:T(2,128)S(1)}, f32[1024,2]{0,1:T(2,128)}, u32[]{:S(2)}) copy-start(f32[1024,2]{0,1:T(2,128)} %param.15) | copy-start | bytes 24580
  268.6 13.3 %copy-start.5 = (bf16[4,4,4,48,384]{4,3,2,1,0:T(8,128)(2,1)S(1)}, bf16[4,4,4,48,384]{4,3,2,1,0:T(8,128)(2,1)}, u32[]{:S(2)}) copy-start(bf16[4,4,4,48,384]{4,3,2,1,0:T(8,128)(2,1)} %get-tuple-element.13) | copy-start | bytes 7077892
  281.9 2.5 copy-start.4
  284.4 2.5 copy-start.3

commit v3 on v2

--- a/solution.py
+++ b/solution.py
@@ -50,22 +50,27 @@
             far = (ids >> 4) ^ fz
             dy = ((ids >> 2) - y) & 3
             dx = (ids - x) & 3
-            slot = jnp.where(dy == 2, 0, jnp.where(dy == 1, 1, jnp.where(dy == 3, 2, 3)))
-            return far * (experts // 2 * capacity) + (slot * 4 + dx) * capacity + at
+            half = at >> 5
+            first = jnp.where(half == 0, dx, dy)
+            then = jnp.where(half == 0, dy, dx)
+            slot = jnp.where(then == 2, 0, jnp.where(then == 1, 1, jnp.where(then == 3, 2, 3)))
+            block = ((far * 4 + slot) * 2 + half) * 4 + first
+            return block * share + (at & (share - 1))
 
         tgt_ref[0:1, :] = row_of(ids0, named0)
         tgt_ref[1:2, :] = row_of(ids1, named1)
         own[...] = jnp.where(named, rank, -1.0).astype(jnp.int32)
-        line = lax.broadcasted_iota(jnp.int32, (share, rows), 0)
         half = share // 2
-        slots = (line + core * share, line + jnp.where(line < half, 0, half) + core * half)
-        for j, dy in enumerate(DYS):
-            for dx in range(4):
-                for dz in range(2):
-                    e = ((fz + dz) % 2) * 16 + ((y + dy) % 4) * 4 + (x + dx) % 4
-                    at = ((j * 4 + dx) * 2 + dz) * share
-                    hit = own[pl.ds(e, 1), :] == slots[dz]
-                    select[at : at + share, :] = jnp.where(hit, 1.0, 0.0).astype(BF)
+        line = lax.broadcasted_iota(jnp.int32, (half, rows), 0) + core * half
+        for h in range(2):
+            for j, then in enumerate(DYS):
+                for first in range(4):
+                    dx, dy = (then, first) if h else (first, then)
+                    for dz in range(2):
+                        e = ((fz + dz) % 2) * 16 + ((y + dy) % 4) * 4 + (x + dx) % 4
+                        at = (((h * 4 + j) * 4 + first) * 2 + dz) * half
+                        hit = own[pl.ds(e, 1), :] == line + h * share
+                        select[at : at + half, :] = jnp.where(hit, 1.0, 0.0).astype(BF)
 
         @pl.loop(0, rows // 64)
         def _(r):
@@ -111,7 +116,9 @@
     )(ids, tokens)
 
 
-def combine_kernel(tgt_ref, w_ref, rows_ref, out_ref, mix):
+def combine_kernel(tgt_ref, w_ref, rows_ref, g_ref, u_ref, d_ref, out_ref, go, uo, do, mix):
+    go[...], uo[...], do[...] = g_ref[...], u_ref[...], d_ref[...]
+
     @pl.when(pl.program_id(0) == 0)
     def _():
         slots = mix.shape[1]
@@ -129,27 +136,33 @@
     out_ref[...] = jnp.dot(mix[...], rows_ref[...], preferred_element_type=F32).astype(BF)
 
 
-def combine(targets, weights, returned):
+def combine(targets, weights, returned, served):
     rows = targets.shape[0]
     slots, width = returned.shape
     block = 512
+    steps = width // block
+    lump = pl.BlockSpec((served[0].shape[0] // steps, served[0].shape[1]), lambda i: (i, 0))
     return pl.pallas_call(
         combine_kernel,
-        grid=(width // block,),
-        out_shape=jax.ShapeDtypeStruct((rows, width), BF),
+        grid=(steps,),
+        out_shape=[jax.ShapeDtypeStruct((rows, width), BF)]
+        + [jax.ShapeDtypeStruct(a.shape, BF) for a in served],
         in_specs=[
             pl.BlockSpec((rows, 2), lambda i: (0, 0)),
             pl.BlockSpec((rows, 2), lambda i: (0, 0)),
             pl.BlockSpec((slots, block), lambda i: (0, i)),
+            lump,
+            lump,
+            lump,
         ],
-        out_specs=pl.BlockSpec((rows, block), lambda i: (0, i)),
+        out_specs=[pl.BlockSpec((rows, block), lambda i: (0, i)), lump, lump, lump],
         scratch_shapes=[pltpu.VMEM((rows, slots), BF)],
         compiler_params=pltpu.CompilerParams(vmem_limit_bytes=48 * MIB),
         cost_estimate=pl.CostEstimate(
             flops=2 * rows * slots * width, bytes_accessed=4 * slots * width, transcendentals=0
         ),
         name="combine",
-    )(targets, weights, returned)
+    )(targets, weights, returned, *served)
 
 
 def exchange_kernel(
@@ -198,29 +211,18 @@
 
     stacks = (wg, wu, wd)
     pieces = [(k, dz) for k in range(3) for dz in (1, 0)]
-    wx_own, wx_in = [], []
+    wx_own, wx_in, wy_own, wy_in, wf_own, wf_in = [], [], [], [], [], []
     for p, (k, dz) in enumerate(pieces):
-        ez = (fz + dz) % 2
-        wx_own.append(near(stacks[k].at[ez, :, x], wx.at[p, x]))
-        wx_in.append(
-            [remote(stacks[k].at[ez, :, (x + dx) % 4], wx.at[p, x], dx=dx) for dx in (2, 1, 3)]
-        )
-    tx_own, tx_in = [], []
-    for j in range(4):
-        to = tx if j < 3 else ty
-        tx_own.append(near(ms.at[j, 0], to.at[j, 0]))
-        tx_in.append([remote(ms.at[j, dx], to.at[j, dx], dx=dx) for dx in (2, 1, 3)])
-
-    wy_own, wy_in, wf_own, wf_in = [], [], [], []
+        stack = stacks[k].at[(fz + dz) % 2]
+        wx_own.append(near(stack.at[:, x], wx.at[p, x]))
+        wx_in.append([remote(stack.at[:, (x + d) % 4], wx.at[p, x], dx=d) for d in (2, 1, 3)])
 
     def weights_y(p):
         wx_own[p].wait()
         for c in wx_in[p]:
             c.wait_recv()
         wy_own.append(near(wx.at[p, :, y], wy.at[p, y]))
-        wy_in.append(
-            [remote(wx.at[p, :, (y + dy) % 4], wy.at[p, y], dy=dy) for dy in (2, 1, 3)]
-        )
+        wy_in.append([remote(wx.at[p, :, (y + d) % 4], wy.at[p, y], dy=d) for d in (2, 1, 3)])
 
     def weights_z(p):
         k, dz = pieces[p]
@@ -232,49 +234,49 @@
         for d in (2,) if dz == 0 else (1, 3):
             wf_in.append(remote(wy.at[p], wf.at[k, z], dz=d))
 
-    ty_in, a_own, a_in, bz_in, b_in = [], [], [], [], []
-
-    def tokens_y(j):
-        tx_own[j].wait()
-        for c in tx_in[j]:
+    axes = (("dx", "dy"), ("dy", "dx"))
+    t1_own, t1_in, t2_in = {}, {}, {}
+    a_own, a_in, bz_in, b_in = {}, {}, {}, {}
+
+    def tokens_first(h, j):
+        to = (tx if j < 3 else ty).at[h, j]
+        t1_own[h, j] = near(ms.at[h, j, 0], to.at[0])
+        t1_in[h, j] = [remote(ms.at[h, j, d], to.at[d], **{axes[h][0]: d}) for d in (2, 1, 3)]
+
+    def tokens_second(h, j):
+        t1_own[h, j].wait()
+        for c in t1_in[h, j]:
             c.wait_recv()
-        ty_in.append(remote(tx.at[j], ty.at[j], dy=DYS[j]))
-
-    def tokens_z(j):
         if j < 3:
-            ty_in[j].wait_recv()
-        else:
-            tx_own[3].wait()
-            for c in tx_in[3]:
-                c.wait_recv()
-        half = ty.shape[3] // 2
-        bz_in.append(
-            [
-                remote(ty.at[j, :, 1, pl.ds(h * half, half)], lhb.at[j, h, :, core], dz=d)
-                for h, d in ((0, 1), (1, 3))
-            ]
-        )
-        a_in.append(remote(ty.at[j, :, 0], lha.at[j, :, core], flip=True))
-        a_own.append(near(ty.at[j, :, 0], lha.at[j, :, core]))
+            t2_in[h, j] = remote(tx.at[h, j], ty.at[h, j], **{axes[h][1]: DYS[j]})
+
+    def tokens_third(j):
+        for h in range(2):
+            if j < 3:
+                t2_in[h, j].wait_recv()
+            bz_in[j, h] = remote(ty.at[h, j, :, 1], lhb.at[j, h, :, core], dz=1 + 2 * h)
+            a_in[j, h] = remote(ty.at[h, j, :, 0], lha.at[j, h, :, core], flip=True)
+            a_own[j, h] = near(ty.at[h, j, :, 0], lha.at[j, h, :, core])
 
     def tokens_b(j):
-        for c in bz_in[j]:
-            c.wait_recv()
-        b_in.append(
-            [remote(lhb.at[j, h, :, core], lhb.at[j, h, :, core], flip=True) for h in range(2)]
-        )
-
+        for h in range(2):
+            bz_in[j, h].wait_recv()
+            b_in[j, h] = remote(lhb.at[j, h, :, core], lhb.at[j, h, :, core], flip=True)
+
+    for j in range(4):
+        tokens_first(0, j)
     weights_y(0)
     for p in range(1, 6):
         weights_y(p)
         weights_z(p - 1)
+    for j in range(4):
+        tokens_first(1, j)
     weights_z(5)
-    tokens_y(0)
-    tokens_y(1)
-    tokens_z(0)
-    tokens_y(2)
-    for j in (1, 2, 3):
-        tokens_z(j)
+    for j in range(4):
+        tokens_second(0, j)
+        tokens_second(1, j)
+    tokens_third(3)
+    tokens_third(0)
 
     for c in wf_own:
         c.wait()
@@ -285,7 +287,21 @@
     width = wf.shape[-1]
     depth = wf.shape[2] * wf.shape[3] * wf.shape[4]
 
-    def expert(rows, i):
+    parts = {}
+    order = []
+
+    def expert(far, j):
+        for h in range(2):
+            if far:
+                b_in[j, h].wait_recv()
+            else:
+                a_own[j, h].wait()
+                a_in[j, h].wait_recv()
+        slot = len(order) % 2
+        if len(order) >= 2:
+            parts[order[-2]].wait_send()
+        order.append((far, j))
+        rows = lhb[j] if far else lha[j]
         v = rows.reshape(-1, rows.shape[-1])
         gate = jnp.dot(v, wf[0].reshape(4 * depth, width), preferred_element_type=F32)
         up = jnp.dot(v, wf[1].reshape(4 * depth, width), preferred_element_type=F32)
@@ -300,107 +316,113 @@
             ).astype(BF).reshape(ps.shape[1:-1] + (depth,))
 
         for s in range(2):
-            ps[i % 2, :, :, :, s * depth : (s + 1) * depth] = part((1 - core) * 2 + s)
-        c = remote(ps.at[i % 2], ra.at[i] if i < 4 else rb.at[i - 4], flip=True)
+            ps[slot, :, :, :, s * depth : (s + 1) * depth] = part((1 - core) * 2 + s)
+        parts[far, j] = remote(ps.at[slot], (rb if far else ra).at[j], flip=True)
         for s in range(2):
-            po[i % 2, :, :, :, s * depth : (s + 1) * depth] = part(core * 2 + s)
-        return c
-
-    parts = []
-    ry_in, rz_in, out_in, out_own = {}, {}, [], []
-
-    def along_x(rows_of, part, j):
-        out_own.append(near(rows_of(0), ret.at[part, j, 0]))
-        for dx in (2, 1, 3):
-            out_in.append(remote(rows_of(dx), ret.at[part, j, dx], dx=4 - dx))
-
-    def near_rows(ref, j):
-        return lambda dx: ref.at[j, dx // 2, pl.ds((dx % 2) * 2, 2)]
-
-    def far_rows(ref, j):
-        return lambda dx: ref.at[j, :, dx]
-
-    def finish(i):
-        parts[i].wait_recv()
-        ref, j = (ra, i) if i < 4 else (rb, i - 4)
-        ref[j] = (ref[j].astype(F32) + po[i % 2].astype(F32)).astype(BF)
-        if i >= 4:
-            rz_in[j] = [remote(rb.at[j, h], rz.at[j, h], dz=d) for h, d in ((0, 3), (1, 1))]
-        elif j < 3:
-            ry_in[j] = remote(ra.at[j], rya.at[j], dy=4 - DYS[j])
+            po[slot, :, :, :, s * depth : (s + 1) * depth] = part(core * 2 + s)
+
+    rq_in, rz_in, out_in, out_own = {}, {}, [], []
+
+    def home(ref, far, j, h):
+        out_own.append(near(ref.at[j, h, 0], ret.at[far, j, h, 0]))
+        for d in (2, 1, 3):
+            out_in.append(
+                remote(ref.at[j, h, d], ret.at[far, j, h, d], **{axes[h][0]: 4 - d})
+            )
+
+    def second(ref, to, far, j, h):
+        if j < 3:
+            rq_in[far, j, h] = remote(ref.at[j, h], to.at[j, h], **{axes[h][1]: 4 - DYS[j]})
         else:
-            along_x(near_rows(ra, 3), 0, 3)
-
-    def near_back(j):
-        ry_in[j].wait_recv()
-        along_x(near_rows(rya, j), 0, j)
-
-    def far_back_y(j):
-        for c in rz_in[j]:
-            c.wait_recv()
-        if j < 3:
-            ry_in[4 + j] = remote(rz.at[j], ryb.at[j], dy=4 - DYS[j])
-        else:
-            along_x(far_rows(rz, 3), 1, 3)
-
-    def far_back_x(j):
-        ry_in[4 + j].wait_recv()
-        along_x(far_rows(ryb, j), 1, j)
-
-    for i in range(8):
-        if i < 4:
-            a_own[i].wait()
-            a_in[i].wait_recv()
-        else:
-            for c in b_in[i - 4]:
-                c.wait_recv()
-        if i >= 2:
-            parts[i - 2].wait_send()
-        parts.append(expert(lha[i] if i < 4 else lhb[i - 4], i))
-        if 3 <= i < 7:
-            tokens_b(i - 3)
-        if i >= 1:
-            finish(i - 1)
-        if 3 <= i < 6:
-            near_back(i - 3)
-    finish(7)
-    far_back_y(0)
-    far_back_y(1)
-    far_back_x(0)
-    far_back_y(2)
-    far_back_y(3)
-    far_back_x(1)
-    far_back_x(2)
+            home(ref, far, j, h)
+
+    def finish(far, j):
+        parts[far, j].wait_recv()
+        ref = rb if far else ra
+        slot = order.index((far, j)) % 2
+        ref[j] = (ref[j].astype(F32) + po[slot].astype(F32)).astype(BF)
+        for h in range(2):
+            if far:
+                rz_in[j, h] = remote(rb.at[j, h], rz.at[j, h], dz=3 - 2 * h)
+            else:
+                second(ra, rya, 0, j, h)
+
+    def near_home(j):
+        for h in range(2):
+            rq_in[0, j, h].wait_recv()
+            home(rya, 0, j, h)
+
+    def far_second(j):
+        for h in range(2):
+            rz_in[j, h].wait_recv()
+            second(rz, ryb, 1, j, h)
+
+    def far_home(j):
+        for h in range(2):
+            rq_in[1, j, h].wait_recv()
+            home(ryb, 1, j, h)
+
+    expert(0, 3)
+    expert(0, 0)
+    finish(0, 3)
+    finish(0, 0)
+    tokens_third(1)
+    tokens_third(2)
+    tokens_b(0)
+    expert(0, 1)
+    expert(0, 2)
+    finish(0, 1)
+    expert(1, 0)
+    finish(0, 2)
+    finish(1, 0)
+    near_home(0)
+    tokens_b(1)
+    tokens_b(2)
+    expert(1, 1)
+    expert(1, 2)
+    finish(1, 1)
+    tokens_b(3)
+    finish(1, 2)
+    near_home(1)
+    near_home(2)
+    far_second(0)
+    expert(1, 3)
+    finish(1, 3)
+    far_second(1)
+    far_second(2)
+    far_home(0)
+    far_second(3)
+    far_home(1)
+    far_home(2)
     for c in out_in:
         c.wait_recv()
     for c in out_own + written:
         c.wait()
-    waited = [id(c) for c in parts[:6]]
+    waited = [id(parts[key]) for key in order[:6]]
     for c in sent:
         if id(c) not in waited:
             c.wait_send()
 
 
 def exchange(mine, gate, up, down):
-    share, model = mine.shape[-2:]
+    half, model = mine.shape[-2:]
     rows, width = gate.shape[-2:]
-    half = share // 2
     cols = model // 2
     hbm = pl.BlockSpec(memory_space=pl.ANY)
     served = jax.ShapeDtypeStruct((4, 4, 4, rows, width), BF)
-    back = (2, 4, share, cols)
+    back = (2, 4, 2 * half, cols)
     return pl.pallas_call(
         exchange_kernel,
-        out_shape=(jax.ShapeDtypeStruct((2, 4, 4, 2, share, cols), BF), served, served, served),
+        out_shape=(jax.ShapeDtypeStruct((2, 4) + back, BF), served, served, served),
         in_specs=[hbm] * 4,
         out_specs=(hbm,) * 4,
         scratch_shapes=[
             pltpu.VMEM((6, 4, 4, rows, width), BF),
             pltpu.VMEM((6, 4, 4, rows, width), BF),
             pltpu.VMEM((3, 4, 4, 4, rows, width), BF),
-            pltpu.VMEM((3, 4, 2, share, model), BF),
-            pltpu.VMEM((4, 4, 2, share, model), BF),
-            pltpu.VMEM((4, 4, 2, share, model), BF),
+            pltpu.VMEM((2, 3, 4, 2, half, model), BF),
+            pltpu.VMEM((2, 4, 4, 2, half, model), BF),
+            pltpu.VMEM((4, 2, 4, 2, half, model), BF),
             pltpu.VMEM((4, 2, 4, 2, half, model), BF),
             pltpu.VMEM((2,) + back, BF),
             pltpu.VMEM((2,) + back, BF),
@@ -409,9 +431,9 @@
             pltpu.VMEM((4,) + back, BF),
             pltpu.VMEM((3,) + back, BF),
             pltpu.VMEM((3,) + back, BF),
-            pltpu.SemaphoreType.DMA((128,)),
-            pltpu.SemaphoreType.DMA((128,)),
-            pltpu.SemaphoreType.DMA((48,)),
+            pltpu.SemaphoreType.DMA((180,)),
+            pltpu.SemaphoreType.DMA((180,)),
+            pltpu.SemaphoreType.DMA((64,)),
         ],
         compiler_params=pltpu.CompilerParams(
             collective_id=0, has_side_effects=True, vmem_limit_bytes=63 * MIB
@@ -436,13 +458,13 @@
     ids = group_pick[None, :] * (experts // GROUPS) + expert_pick.T
     mine, targets = dispatch(ids, tokens, experts, share)
     returned, gate_new, up_new, down_new = exchange(
-        mine.reshape(4, 4, 2, share, model_width), gate, up, down
+        mine.reshape(2, 4, 4, 2, share // 2, model_width), gate, up, down
     )
-    combined = combine(
-        targets.T, route_weight, returned.reshape(experts * capacity, model_width // 2)
+    served = [a.reshape(model_width, width) for a in (gate_new, up_new, down_new)]
+    combined, *served = combine(
+        targets.T, route_weight, returned.reshape(experts * capacity, model_width // 2), served
     )
-    whole = (1, model_width, width)
-    return (combined, gate_new.reshape(whole), up_new.reshape(whole), down_new.reshape(whole))
+    return (combined, *(a[None] for a in served))
 
 
 def solution(mesh):

time: 290 us -> 246 us (0.85)
  Pallas kernels: 276 us -> 231 us
  other arithmetic: 4.42 us -> 7.98 us
    pallas_call x2, Pallas kernels: 261 us -> 215 us  [the longest x1 201 us: exchange(): pl.pallas_call(exchange_kernel, out_shape=(jax.ShapeDtypeStruct((2, 4) +...]
    unnamed x20 -> x11, local copies, waits for them, and re-layouts: 6.95 us -> 5.28 us
where the time goes in v3:
time: 246 us; the launch traced here: 245 us
  Pallas kernels  231 us (94%)
  other arithmetic  7.98 us (3%)
  local copies, waits for them, and re-layouts  6.31 us (3%)
    pallas_call x1, Pallas kernels, exchange(): pl.pallas_call(exchange_kernel, out_shape=(jax.ShapeDtypeStruct((2, 4) +...  201 us
    pallas_call x1, Pallas kernels, dispatch(): pl.pallas_call(functools.partial(dispatch_kernel, experts, share), grid=(...  15.2 us
    pallas_call x1, Pallas kernels, combine(): pl.pallas_call(combine_kernel, grid=(steps,), out_shape=[jax.ShapeDtypeSt...  14.2 us
    unnamed x11, local copies, waits for them, and re-layouts  5.28 us

profile of v3, /device:TPU:1, one launch (start us, length us, event | category | flops | bytes accessed | tf_op | source)
XLA Modules:
  0.0 245.5 jit_solution(6487995336895155853)
XLA Ops:
  0.6 0.0 copy-start.3
  0.6 0.0 copy-start.4
  0.7 0.8 broadcast_multiply_fusion
  1.5 0.7 add_bitcast_fusion.ids_ref
  2.2 0.9 copy.13.w_ref
  3.1 2.8 %convert_element_type.11 = bf16[32,48,384]{2,1,0:T(8,128)(2,1)} convert(f32[32,48,384]{2,1,0:T(8,128)} %param.12) | non-fusion elementwise | flops 589824 | bytes 3538944 | tf_op jit(solution)/shard_map/convert_element_type | solution.py:453
  5.9 0.0 copy-done.3
  5.9 0.0 copy-done.4
  5.9 3.6 %multiply_convert_fusion = (bf16[32,48,384]{2,1,0:T(8,128)(2,1)}, bf16[32,48,384]{2,1,0:T(8,128)(2,1)}) fusion(f32[32,48,384]{2,1,0:T(8,128)S(1)} %copy-done.3, f32[48]{0:T(128)S(1)} %copy-done.4, f32[32,48,384]{2,1,0:T(8,128)} %param.10), kind=kLoop, calls=%fused_computation | loop fusion | flops 2359296 | bytes 7078080 | tf_op jit(solution)/shard_map/convert_element_type | solution.py:452
  9.6 15.2 %dispatch.1 = (bf16[1024,3072]{1,0:T(8,128)(2,1)}, s32[2,1024]{1,0:T(2,128)S(1)}) custom-call(s32[2,1024]{1,0:T(2,128)S(1)} %add_bitcast_fusion.ids_ref, bf16[1024,3072]{1,0:T(8,128)(2,1)} %tok_ref.1), custom_call_target="tpu_custom_call" | custom-call | flops 6442450944 | bytes 12582912 | tf_op jit(solution)/shard_map/dispatch/pallas_call | solution.py:89
  24.8 1.0 copy.12
  25.8 201.1 %exchange.1 = (bf16[2,4,2,4,32,1536]{5,4,3,2,1,0:T(8,128)(2,1)}, bf16[4,4,4,48,384]{4,3,2,1,0:T(8,128)(2,1)}, bf16[4,4,4,48,384]{4,3,2,1,0:T(8,128)(2,1)}, bf16[4,4,4,48,384]{4,3,2,1,0:T(8,128)(2,1)}) custom-call(bf16[2,4,4,2,16,3072]{5,4,3,2,1,0:T(8,128)(2,1)} %bitcast.17, bf16[2,4,4,48,384]{4,3,2,1,0:T(8,128)(2,1)} %bitcast.20, ...), custom_call_target="tpu_custom_call" | custom-call | tf_op jit(solution)/shard_map/exchange/pallas_call | solution.py:414
  226.9 0.0 copy-start
  226.9 1.0 copy-done
  228.0 0.0 copy-start.1
  228.0 1.7 copy-done.1
  229.6 0.0 copy-start.2
  229.6 1.7 copy-done.2
  231.3 14.2 %combine.1 = (bf16[1024,1536]{1,0:T(8,128)(2,1)}, bf16[3072,384]{1,0:T(8,128)(2,1)}, bf16[3072,384]{1,0:T(8,128)(2,1)}, bf16[3072,384]{1,0:T(8,128)(2,1)}) custom-call(s32[1024,2]{1,0:T(8,128)S(1)} %bitcast.14, f32[1024,2]{1,0:T(8,128)S(1)} %copy.13.w_ref, bf16[2048,1536]{1,0:T(8,128)(2,1)} %bitcast.21, bf16[3072,384]{1,0:T(8,128)(2,1)S(1)} %bitcast.15, ...), custom_call_target="tpu_custom_call" | custom-call | flops 6442450944 | bytes 12582912 | tf_op jit(solution)/shard_map/combine/pallas_call | solution.py:145
Async XLA Ops:
  0.6 5.3 %copy-start.3 = (f32[32,48,384]{2,1,0:T(8,128)S(1)}, f32[32,48,384]{2,1,0:T(8,128)}, u32[]{:S(2)}) copy-start(f32[32,48,384]{2,1,0:T(8,128)} %param.11) | copy-start | bytes 7077892
  0.6 5.3 %copy-start.4 = (f32[48]{0:T(128)S(1)}, f32[48]{0:T(128)}, u32[]{:S(2)}) copy-start(f32[48]{0:T(128)} %param.9) | copy-start | bytes 580
  226.9 1.0 copy-start
  228.0 1.7 copy-start.1
  229.6 1.7 copy-start.2

commit v4 on v3

--- a/solution.py
+++ b/solution.py
@@ -22,122 +22,30 @@
     return lax.axis_index("gr") * 2 + fz, fz, y, x, lax.axis_index("tp")
 
 
-def dispatch_kernel(experts, share, ids_ref, tok_ref, out_ref, tgt_ref, select, normed, own):
-    rows = tok_ref.shape[0]
-    width = out_ref.shape[1]
-    step = pl.program_id(0)
-
-    @pl.when(step == 0)
-    def _():
-        _, fz, y, x, core = place()
-        ids0, ids1 = ids_ref[0:1, :], ids_ref[1:2, :]
-        which = lax.broadcasted_iota(jnp.int32, (experts, rows), 0)
-        named0, named1 = ids0 == which, ids1 == which
-        named = named0 | named1
-        before = (
-            lax.broadcasted_iota(jnp.int32, (rows, rows), 0)
-            < lax.broadcasted_iota(jnp.int32, (rows, rows), 1)
-        )
-        rank = jnp.dot(
-            jnp.where(named, 1.0, 0.0).astype(BF),
-            jnp.where(before, 1.0, 0.0).astype(BF),
-            preferred_element_type=F32,
-        )
-        capacity = 2 * share
-
-        def row_of(ids, named_k):
-            at = jnp.sum(jnp.where(named_k, rank, 0.0), axis=0, keepdims=True).astype(jnp.int32)
-            far = (ids >> 4) ^ fz
-            dy = ((ids >> 2) - y) & 3
-            dx = (ids - x) & 3
-            half = at >> 5
-            first = jnp.where(half == 0, dx, dy)
-            then = jnp.where(half == 0, dy, dx)
-            slot = jnp.where(then == 2, 0, jnp.where(then == 1, 1, jnp.where(then == 3, 2, 3)))
-            block = ((far * 4 + slot) * 2 + half) * 4 + first
-            return block * share + (at & (share - 1))
-
-        tgt_ref[0:1, :] = row_of(ids0, named0)
-        tgt_ref[1:2, :] = row_of(ids1, named1)
-        own[...] = jnp.where(named, rank, -1.0).astype(jnp.int32)
-        half = share // 2
-        line = lax.broadcasted_iota(jnp.int32, (half, rows), 0) + core * half
-        for h in range(2):
-            for j, then in enumerate(DYS):
-                for first in range(4):
-                    dx, dy = (then, first) if h else (first, then)
-                    for dz in range(2):
-                        e = ((fz + dz) % 2) * 16 + ((y + dy) % 4) * 4 + (x + dx) % 4
-                        at = (((h * 4 + j) * 4 + first) * 2 + dz) * half
-                        hit = own[pl.ds(e, 1), :] == line + h * share
-                        select[at : at + half, :] = jnp.where(hit, 1.0, 0.0).astype(BF)
-
-        @pl.loop(0, rows // 64)
-        def _(r):
-            at = pl.ds(pl.multiple_of(r * 64, 64), 64)
-            v = tok_ref[at, :].astype(F32)
-            scale = lax.rsqrt(jnp.mean(v * v, axis=-1, keepdims=True) + EPS)
-            normed[at, :] = (v * scale).astype(BF)
-
-    cols = pl.ds(pl.multiple_of(step * width, width), width)
-    out_ref[...] = jnp.dot(select[...], normed[:, cols], preferred_element_type=F32).astype(BF)
-
-
-def dispatch(ids, tokens, experts, share):
-    rows, width = tokens.shape
-    block = 512
-    return pl.pallas_call(
-        functools.partial(dispatch_kernel, experts, share),
-        grid=(width // block,),
-        out_shape=(
-            jax.ShapeDtypeStruct((experts * share, width), BF),
-            jax.ShapeDtypeStruct((2, rows), jnp.int32),
-        ),
-        in_specs=[
-            pl.BlockSpec((2, rows), lambda i: (0, 0)),
-            pl.BlockSpec((rows, width), lambda i: (0, 0)),
-        ],
-        out_specs=(
-            pl.BlockSpec((experts * share, block), lambda i: (0, i)),
-            pl.BlockSpec((2, rows), lambda i: (0, 0)),
-        ),
-        scratch_shapes=[
-            pltpu.VMEM((experts * share, rows), BF),
-            pltpu.VMEM((rows, width), BF),
-            pltpu.VMEM((experts, rows), jnp.int32),
-        ],
-        compiler_params=pltpu.CompilerParams(vmem_limit_bytes=48 * MIB),
-        cost_estimate=pl.CostEstimate(
-            flops=2 * experts * share * rows * width,
-            bytes_accessed=4 * rows * width,
-            transcendentals=0,
-        ),
-        name="dispatch",
-    )(ids, tokens)
-
-
-def combine_kernel(tgt_ref, w_ref, rows_ref, g_ref, u_ref, d_ref, out_ref, go, uo, do, mix):
+def combine_kernel(table_ref, rows_ref, g_ref, u_ref, d_ref, out_ref, go, uo, do, mix, table):
     go[...], uo[...], do[...] = g_ref[...], u_ref[...], d_ref[...]
 
     @pl.when(pl.program_id(0) == 0)
     def _():
         slots = mix.shape[1]
         tile = 128
+        table[...] = table_ref[...].T
 
         @pl.loop(0, mix.shape[0] // tile)
         def _(r):
             at = pl.ds(pl.multiple_of(r * tile, tile), tile)
             slot = lax.broadcasted_iota(jnp.int32, (tile, slots), 1)
-            t, w = tgt_ref[at, :], w_ref[at, :]
+            t = table[at, :]
+            row = t.astype(jnp.int32)
             mix[at, :] = jnp.where(
-                slot == t[:, 0:1], w[:, 0:1], jnp.where(slot == t[:, 1:2], w[:, 1:2], 0.0)
+                slot == row[:, 0:1], t[:, 2:3], jnp.where(slot == row[:, 1:2], t[:, 3:4], 0.0)
             ).astype(BF)
 
     out_ref[...] = jnp.dot(mix[...], rows_ref[...], preferred_element_type=F32).astype(BF)
 
 
-def combine(targets, weights, returned, served):
-    rows = targets.shape[0]
+def combine(table, returned, served):
+    lines, rows = table.shape
     slots, width = returned.shape
     block = 512
     steps = width // block
@@ -148,28 +56,30 @@
         out_shape=[jax.ShapeDtypeStruct((rows, width), BF)]
         + [jax.ShapeDtypeStruct(a.shape, BF) for a in served],
         in_specs=[
-            pl.BlockSpec((rows, 2), lambda i: (0, 0)),
-            pl.BlockSpec((rows, 2), lambda i: (0, 0)),
+            pl.BlockSpec((lines, rows), lambda i: (0, 0)),
             pl.BlockSpec((slots, block), lambda i: (0, i)),
             lump,
             lump,
             lump,
         ],
         out_specs=[pl.BlockSpec((rows, block), lambda i: (0, i)), lump, lump, lump],
-        scratch_shapes=[pltpu.VMEM((rows, slots), BF)],
-        compiler_params=pltpu.CompilerParams(vmem_limit_bytes=48 * MIB),
+        scratch_shapes=[pltpu.VMEM((rows, slots), BF), pltpu.VMEM((rows, lines), F32)],
+        compiler_params=pltpu.CompilerParams(vmem_limit_bytes=63 * MIB),
         cost_estimate=pl.CostEstimate(
             flops=2 * rows * slots * width, bytes_accessed=4 * slots * width, transcendentals=0
         ),
         name="combine",
-    )(targets, weights, returned, *served)
+    )(table, returned, *served)
 
 
 def exchange_kernel(
-    ms, wg, wu, wd, ret, og, ou, od,
-    wx, wy, wf, tx, ty, lha, lhb, ps, po, ra, rb, rz, rya, ryb, send, recv, here,
+    group, picks, scales, tokens, wg, wu, wd, ret, og, ou, od, ms, table,
+    wx, wy, wf, tx, ty, lha, lhb, ps, po, pool, select, own, stage, send, recv, here, ready,
 ):
     z, fz, y, x, core = place()
+    ra, rb, rz, rya, ryb = (
+        pool.at[pl.ds(at, n)] for at, n in ((0, 4), (4, 4), (8, 4), (12, 3), (15, 3))
+    )
     used = {"away": 0, "near": 0}
     sent, local_copies = [], []
 
@@ -217,6 +127,104 @@
         wx_own.append(near(stack.at[:, x], wx.at[p, x]))
         wx_in.append([remote(stack.at[:, (x + d) % 4], wx.at[p, x], dx=d) for d in (2, 1, 3)])
 
+    cols = pool.shape[-1]
+    loads = [
+        near(tokens.at[b, :, :, :, pl.ds(s * cols, cols)], pool.at[s * 4 + b])
+        for b in range(4)
+        for s in range(2)
+    ]
+
+    def route():
+        rows = group.shape[1]
+        experts = own.shape[0]
+        per_group = experts // GROUPS
+        share = ms.shape[-2] * 2
+        half = share // 2
+        ids0 = group[...] * per_group + picks[0:1, :]
+        ids1 = group[...] * per_group + picks[1:2, :]
+        which = lax.broadcasted_iota(jnp.int32, (experts, rows), 0)
+        named0, named1 = ids0 == which, ids1 == which
+        named = named0 | named1
+        before = (
+            lax.broadcasted_iota(jnp.int32, (rows, rows), 0)
+            < lax.broadcasted_iota(jnp.int32, (rows, rows), 1)
+        )
+        rank = jnp.dot(
+            jnp.where(named, 1.0, 0.0).astype(BF),
+            jnp.where(before, 1.0, 0.0).astype(BF),
+            preferred_element_type=F32,
+        )
+
+        def row_of(ids, named_k):
+            at = jnp.sum(jnp.where(named_k, rank, 0.0), axis=0, keepdims=True).astype(jnp.int32)
+            far = (ids >> 4) ^ fz
+            dy = ((ids >> 2) - y) & 3
+            dx = (ids - x) & 3
+            h = at >> 5
+            first = jnp.where(h == 0, dx, dy)
+            then = jnp.where(h == 0, dy, dx)
+            slot = jnp.where(then == 2, 0, jnp.where(then == 1, 1, jnp.where(then == 3, 2, 3)))
+            block = ((far * 4 + slot) * 2 + h) * 4 + first
+            return (block * share + (at & (share - 1))).astype(F32)
+
+        table[0:1, :] = row_of(ids0, named0)
+        table[1:2, :] = row_of(ids1, named1)
+        table[2:4, :] = scales[...]
+        table[4:8, :] = jnp.zeros((4, rows), F32)
+        own[...] = jnp.where(named, rank, -1.0).astype(jnp.int32)
+        line = lax.broadcasted_iota(jnp.int32, (half, rows), 0) + core * half
+        for h in range(2):
+            for j, then in enumerate(DYS):
+                for first in range(4):
+                    dx, dy = (then, first) if h else (first, then)
+                    for dz in range(2):
+                        e = ((fz + dz) % 2) * 16 + ((y + dy) % 4) * 4 + (x + dx) % 4
+                        at = (((h * 4 + j) * 4 + first) * 2 + dz) * half
+                        hit = own[pl.ds(e, 1), :] == line + h * share
+                        select[at : at + half, :] = jnp.where(hit, 1.0, 0.0).astype(BF)
+
+    def normalize():
+        for c in loads:
+            c.wait()
+
+        @pl.loop(0, 4)
+        def _(b):
+            for u in range(2):
+                for w in range(2):
+                    at = (u, pl.ds(w * 2, 2))
+                    left = pool[(b,) + at].astype(F32)
+                    right = pool[(4 + b,) + at].astype(F32)
+                    total = jnp.sum(left * left, axis=-1, keepdims=True) + jnp.sum(
+                        right * right, axis=-1, keepdims=True
+                    )
+                    scale = lax.rsqrt(total * (1.0 / (2 * cols)) + EPS)
+                    pool[(b,) + at] = (left * scale).astype(BF)
+                    pool[(4 + b,) + at] = (right * scale).astype(BF)
+
+    placed = []
+    block = stage.shape[-1]
+    steps = cols // block
+
+    def tile(t):
+        s, n = t // steps, t % steps
+        if t >= 2:
+            placed[t - 2].wait()
+        rows = pool[s * 4 : s * 4 + 4, :, :, :, n * block : (n + 1) * block]
+        stage[t % 2] = (
+            jnp.dot(select[...], rows.reshape(-1, block), preferred_element_type=F32)
+            .astype(BF)
+            .reshape(stage.shape[1:])
+        )
+        placed.append(
+            near(stage.at[t % 2], ms.at[:, :, :, :, :, pl.ds(s * cols + n * block, block)])
+        )
+
+    def tokens_ready():
+        for c in placed[-2:]:
+            c.wait()
+        for to in peers:
+            pl.semaphore_signal(ready, inc=1, device_id=device(**to), device_id_type=MESH)
+
     def weights_y(p):
         wx_own[p].wait()
         for c in wx_in[p]:
@@ -263,10 +271,23 @@
             bz_in[j, h].wait_recv()
             b_in[j, h] = remote(lhb.at[j, h, :, core], lhb.at[j, h, :, core], flip=True)
 
+    route()
+    normalize()
+    tile(0)
+    weights_y(0)
+    tile(1)
+    tile(2)
+    weights_y(1)
+    weights_z(0)
+    tile(3)
+    tile(4)
+    weights_y(2)
+    weights_z(1)
+    tile(5)
+    tokens_ready()
     for j in range(4):
         tokens_first(0, j)
-    weights_y(0)
-    for p in range(1, 6):
+    for p in range(3, 6):
         weights_y(p)
         weights_z(p - 1)
     for j in range(4):
@@ -278,6 +299,7 @@
     tokens_third(3)
     tokens_third(0)
 
+    pl.semaphore_wait(ready, len(peers))
     for c in wf_own:
         c.wait()
     for c in wf_in:
@@ -404,18 +426,29 @@
             c.wait_send()
 
 
-def exchange(mine, gate, up, down):
-    half, model = mine.shape[-2:]
+def exchange(group, picks, scales, tokens, gate, up, down):
+    model = tokens.shape[-1]
+    total = tokens.size // model
     rows, width = gate.shape[-2:]
+    experts = gate.shape[0] * gate.shape[1] * gate.shape[2]
+    half = picks.shape[0] * total // experts // 4
     cols = model // 2
     hbm = pl.BlockSpec(memory_space=pl.ANY)
+    vmem = pl.BlockSpec(memory_space=pltpu.VMEM)
     served = jax.ShapeDtypeStruct((4, 4, 4, rows, width), BF)
     back = (2, 4, 2 * half, cols)
     return pl.pallas_call(
         exchange_kernel,
-        out_shape=(jax.ShapeDtypeStruct((2, 4) + back, BF), served, served, served),
-        in_specs=[hbm] * 4,
-        out_specs=(hbm,) * 4,
+        out_shape=(
+            jax.ShapeDtypeStruct((2, 4) + back, BF),
+            served,
+            served,
+            served,
+            jax.ShapeDtypeStruct((2, 4, 4, 2, half, model), BF),
+            jax.ShapeDtypeStruct((8, total), F32),
+        ),
+        in_specs=[vmem] * 3 + [hbm] * 4,
+        out_specs=(hbm,) * 5 + (vmem,),
         scratch_shapes=[
             pltpu.VMEM((6, 4, 4, rows, width), BF),
             pltpu.VMEM((6, 4, 4, rows, width), BF),
@@ -426,20 +459,20 @@
             pltpu.VMEM((4, 2, 4, 2, half, model), BF),
             pltpu.VMEM((2,) + back, BF),
             pltpu.VMEM((2,) + back, BF),
-            pltpu.VMEM((4,) + back, BF),
-            pltpu.VMEM((4,) + back, BF),
-            pltpu.VMEM((4,) + back, BF),
-            pltpu.VMEM((3,) + back, BF),
-            pltpu.VMEM((3,) + back, BF),
+            pltpu.VMEM((18,) + back, BF),
+            pltpu.VMEM((experts * 2 * half, total), BF),
+            pltpu.VMEM((experts, total), jnp.int32),
+            pltpu.VMEM((2, 2, 4, 4, 2, half, 512), BF),
             pltpu.SemaphoreType.DMA((180,)),
             pltpu.SemaphoreType.DMA((180,)),
-            pltpu.SemaphoreType.DMA((64,)),
+            pltpu.SemaphoreType.DMA((72,)),
+            pltpu.SemaphoreType.REGULAR,
         ],
         compiler_params=pltpu.CompilerParams(
-            collective_id=0, has_side_effects=True, vmem_limit_bytes=63 * MIB
+            collective_id=0, has_side_effects=True, vmem_limit_bytes=67_000_000
         ),
         name="exchange",
-    )(mine, gate, up, down)
+    )(group, picks, scales, tokens, gate, up, down)
 
 
 def local(
@@ -452,17 +485,18 @@
     up = (scaled * up_weight).astype(BF).reshape(split)
     down = down_weight.astype(BF).reshape(split)
     tok_rows, model_width = tokens.shape
-    top_count = expert_pick.shape[1]
-    capacity = top_count * tok_rows // experts
-    share = capacity // 2
-    ids = group_pick[None, :] * (experts // GROUPS) + expert_pick.T
-    mine, targets = dispatch(ids, tokens, experts, share)
-    returned, gate_new, up_new, down_new = exchange(
-        mine.reshape(2, 4, 4, 2, share // 2, model_width), gate, up, down
+    returned, gate_new, up_new, down_new, _, table = exchange(
+        group_pick[None, :],
+        expert_pick.T,
+        route_weight.T,
+        tokens.reshape(4, 2, 4, tok_rows // 32, model_width),
+        gate,
+        up,
+        down,
     )
     served = [a.reshape(model_width, width) for a in (gate_new, up_new, down_new)]
     combined, *served = combine(
-        targets.T, route_weight, returned.reshape(experts * capacity, model_width // 2), served
+        table, returned.reshape(expert_pick.shape[1] * tok_rows, model_width // 2), served
     )
     return (combined, *(a[None] for a in served))
 

time: 246 us -> 225 us (0.915)
  Pallas kernels: 231 us -> 218 us
  local copies, waits for them, and re-layouts: 6.31 us -> 0.01 us
    pallas_call x1 -> x0, Pallas kernels: 15.2 us -> none  [dispatch(): pl.pallas_call(functools.partial(dispatch_kernel, experts, share), grid=(...]
    unnamed x11 -> x4, local copies, waits for them, and re-layouts: 5.28 us -> 0.01 us
where the time goes in v4:
time: 225 us
  Pallas kernels  218 us (97%)
  other arithmetic  6.46 us (3%)
    pallas_call x1, Pallas kernels, exchange(): pl.pallas_call(exchange_kernel, out_shape=(jax.ShapeDtypeStruct((2, 4) +...  203 us
    pallas_call x1, Pallas kernels, combine(): pl.pallas_call(combine_kernel, grid=(steps,), out_shape=[jax.ShapeDtypeSt...  15.2 us

profile of v4, /device:TPU:1, one launch (start us, length us, event | category | flops | bytes accessed | tf_op | source)
XLA Modules:
  0.0 225.2 jit_solution(2675460304248587365)
XLA Ops:
  0.6 0.0 copy-start
  0.6 0.0 copy-start.1
  0.7 3.0 %convert_element_type.11 = bf16[32,48,384]{2,1,0:T(8,128)(2,1)} convert(f32[32,48,384]{2,1,0:T(8,128)} %param.12) | non-fusion elementwise | flops 589824 | bytes 3538944 | tf_op jit(solution)/shard_map/convert_element_type | solution.py:486
  3.6 0.0 copy-done
  3.6 0.0 copy-done.1
  3.6 3.5 %multiply_convert_fusion = (bf16[32,48,384]{2,1,0:T(8,128)(2,1)}, bf16[32,48,384]{2,1,0:T(8,128)(2,1)}) fusion(f32[32,48,384]{2,1,0:T(8,128)S(1)} %copy-done, f32[48]{0:T(128)S(1)} %copy-done.1, f32[32,48,384]{2,1,0:T(8,128)} %param.10), kind=kLoop, calls=%fused_computation | loop fusion | flops 2359296 | bytes 7078080 | tf_op jit(solution)/shard_map/convert_element_type | solution.py:485
  7.1 202.6 %exchange.1 = (bf16[2,4,2,4,32,1536]{5,4,3,2,1,0:T(8,128)(2,1)}, bf16[4,4,4,48,384]{4,3,2,1,0:T(8,128)(2,1)}, bf16[4,4,4,48,384]{4,3,2,1,0:T(8,128)(2,1)}, bf16[...) custom-call(s32[1,1024]{1,0:T(1,128)} %bitcast.20, ...), custom_call_target="tpu_custom_call" | custom-call | tf_op jit(solution)/shard_map/exchange/pallas_call | solution.py:440
  209.7 15.2 %combine.1 = (bf16[1024,1536]{1,0:T(8,128)(2,1)}, bf16[3072,384]{1,0:T(8,128)(2,1)}, bf16[3072,384]{1,0:T(8,128)(2,1)}, bf16[3072,384]{1,0:T(8,128)(2,1)}) custom-call(f32[8,1024]{1,0:T(8,128)} %get-tuple-element.13.table_ref, bf16[2048,1536]{1,0:T(8,128)(2,1)} %bitcast.21, bf16[3072,384]{1,0:T(8,128)(2,1)} %bitcast.22, bf16[3072,384]{1,0:T(8,128)(2,1)} %bitcast.23, ...), custom_call_target="tpu_custom_call" | custom-call | flops 6442450944 | bytes 12582912 | tf_op jit(solution)/shard_map/combine/pallas_call | solution.py:53
Async XLA Ops:
  0.6 3.0 %copy-start = (f32[32,48,384]{2,1,0:T(8,128)S(1)}, f32[32,48,384]{2,1,0:T(8,128)}, u32[]{:S(2)}) copy-start(f32[32,48,384]{2,1,0:T(8,128)} %param.11) | copy-start | bytes 7077892
  0.6 3.0 %copy-start.1 = (f32[48]{0:T(128)S(1)}, f32[48]{0:T(128)}, u32[]{:S(2)}) copy-start(f32[48]{0:T(128)} %param.9) | copy-start | bytes 580

commit v5 on v4

--- a/solution.py
+++ b/solution.py
@@ -73,12 +73,12 @@
 
 
 def exchange_kernel(
-    group, picks, scales, tokens, wg, wu, wd, ret, og, ou, od, ms, table,
-    wx, wy, wf, tx, ty, lha, lhb, ps, po, pool, select, own, stage, send, recv, here, ready,
+    group, picks, scales, gain, tokens, wg, wu, wd, ret, og, ou, od, ms, table,
+    wide, ws, wx, wy, wf, tx, ty, lha, lhb, ps, po, pool, own, send, recv, here, ready,
 ):
     z, fz, y, x, core = place()
-    ra, rb, rz, rya, ryb = (
-        pool.at[pl.ds(at, n)] for at, n in ((0, 4), (4, 4), (8, 4), (12, 3), (15, 3))
+    ra, rb, rz, rya = (
+        pool.at[pl.ds(at, n)] for at, n in ((0, 4), (4, 4), (8, 4), (12, 3))
     )
     used = {"away": 0, "near": 0}
     sent, local_copies = [], []
@@ -113,19 +113,39 @@
         c.start()
         return c
 
+    stacks = (wg, wu, wd)
+    pieces = [(k, dz) for k in range(3) for dz in (1, 0)]
+    cast_order = (0, 4, 1, 5, 2, 3)
+    wx_own, wx_in, wy_in, wf_own, wf_in = {}, {}, {}, [], []
+
+    def fetch(q):
+        k, dz = pieces[cast_order[q // 2]]
+        return near(stacks[k].at[(fz + dz) % 2, pl.ds(q % 2 * 2, 2)], wide.at[q % 2])
+
+    fetched = [fetch(0), fetch(1)]
     barrier = pltpu.get_barrier_semaphore()
     peers = [{"flip": True}] + [{axis: d} for axis in ("dz", "dy", "dx") for d in (1, 2, 3)]
-    for to in peers:
+    corners = [{"dy": i, "dx": j} for i in (1, 2, 3) for j in (1, 2, 3)]
+    for to in peers + corners:
         pl.semaphore_signal(barrier, inc=1, device_id=device(**to), device_id_type=MESH)
-    pl.semaphore_wait(barrier, len(peers))
-
-    stacks = (wg, wu, wd)
-    pieces = [(k, dz) for k in range(3) for dz in (1, 0)]
-    wx_own, wx_in, wy_own, wy_in, wf_own, wf_in = [], [], [], [], [], []
-    for p, (k, dz) in enumerate(pieces):
-        stack = stacks[k].at[(fz + dz) % 2]
-        wx_own.append(near(stack.at[:, x], wx.at[p, x]))
-        wx_in.append([remote(stack.at[:, (x + d) % 4], wx.at[p, x], dx=d) for d in (2, 1, 3)])
+    for i, p in enumerate(cast_order):
+        k = pieces[p][0]
+        for q in (2 * i, 2 * i + 1):
+            fetched[q].wait()
+            v = wide[q % 2]
+            ws[p, q % 2 * 2 : q % 2 * 2 + 2] = (
+                v if k == 2 else gain[...][None, None] * v
+            ).astype(BF)
+            if q + 2 < 2 * len(pieces):
+                fetched.append(fetch(q + 2))
+        if i == 0:
+            pl.semaphore_wait(barrier, len(peers + corners))
+        if p < 4:
+            wx_own[p] = near(ws.at[p, :, x], wx.at[p, x])
+            wx_in[p] = [remote(ws.at[p, :, (x + d) % 4], wx.at[p, x], dx=d) for d in (2, 1, 3)]
+        else:
+            wx_own[p] = near(ws.at[p, y], wx.at[p, y])
+            wx_in[p] = [remote(ws.at[p, (y + d) % 4], wx.at[p, y], dy=d) for d in (2, 1, 3)]
 
     cols = pool.shape[-1]
     loads = [
@@ -138,22 +158,26 @@
         rows = group.shape[1]
         experts = own.shape[0]
         per_group = experts // GROUPS
-        share = ms.shape[-2] * 2
+        share = ms.shape[-2]
         half = share // 2
         ids0 = group[...] * per_group + picks[0:1, :]
         ids1 = group[...] * per_group + picks[1:2, :]
         which = lax.broadcasted_iota(jnp.int32, (experts, rows), 0)
         named0, named1 = ids0 == which, ids1 == which
         named = named0 | named1
-        before = (
-            lax.broadcasted_iota(jnp.int32, (rows, rows), 0)
-            < lax.broadcasted_iota(jnp.int32, (rows, rows), 1)
-        )
-        rank = jnp.dot(
-            jnp.where(named, 1.0, 0.0).astype(BF),
-            jnp.where(before, 1.0, 0.0).astype(BF),
-            preferred_element_type=F32,
-        )
+        counted = jnp.where(named, 1.0, 0.0).astype(BF)
+        lump = 256
+        rank = jnp.zeros(named.shape, F32)
+        for at in range(0, rows, lump):
+            before = (
+                lax.broadcasted_iota(jnp.int32, (lump, rows), 0) + at
+                < lax.broadcasted_iota(jnp.int32, (lump, rows), 1)
+            )
+            rank += jnp.dot(
+                counted[:, at : at + lump],
+                jnp.where(before, 1.0, 0.0).astype(BF),
+                preferred_element_type=F32,
+            )
 
         def row_of(ids, named_k):
             at = jnp.sum(jnp.where(named_k, rank, 0.0), axis=0, keepdims=True).astype(jnp.int32)
@@ -181,7 +205,8 @@
                         e = ((fz + dz) % 2) * 16 + ((y + dy) % 4) * 4 + (x + dx) % 4
                         at = (((h * 4 + j) * 4 + first) * 2 + dz) * half
                         hit = own[pl.ds(e, 1), :] == line + h * share
-                        select[at : at + half, :] = jnp.where(hit, 1.0, 0.0).astype(BF)
+                        line_at = (at // 256 + 8, at // 128 % 2, at // 32 % 4, pl.ds(at % 32, half))
+                        pool[line_at + (slice(0, rows),)] = jnp.where(hit, 1.0, 0.0).astype(BF)
 
     def normalize():
         for c in loads:
@@ -202,22 +227,18 @@
                     pool[(4 + b,) + at] = (right * scale).astype(BF)
 
     placed = []
-    block = stage.shape[-1]
-    steps = cols // block
 
     def tile(t):
-        s, n = t // steps, t % steps
+        s, m = t // 4, t % 4
         if t >= 2:
             placed[t - 2].wait()
-        rows = pool[s * 4 : s * 4 + 4, :, :, :, n * block : (n + 1) * block]
-        stage[t % 2] = (
-            jnp.dot(select[...], rows.reshape(-1, block), preferred_element_type=F32)
-            .astype(BF)
-            .reshape(stage.shape[1:])
+        rows = pool[s * 4 : s * 4 + 4].reshape(-1, cols)
+        select = pool[8 + m, :, :, :, : group.shape[1]].reshape(-1, group.shape[1])
+        ps[t % 2] = (
+            jnp.dot(select, rows, preferred_element_type=F32).astype(BF).reshape(ps.shape[1:])
         )
-        placed.append(
-            near(stage.at[t % 2], ms.at[:, :, :, :, :, pl.ds(s * cols + n * block, block)])
-        )
+        to = ms.at[m // 2, pl.ds(m % 2 * 2, 2), :, :, pl.ds(s * cols, cols)]
+        placed.append(near(ps.at[t % 2], to))
 
     def tokens_ready():
         for c in placed[-2:]:
@@ -225,22 +246,29 @@
         for to in peers:
             pl.semaphore_signal(ready, inc=1, device_id=device(**to), device_id_type=MESH)
 
+    def weights_up(p, block, at):
+        k, dz = pieces[p]
+        to = wf.at[k, z, at] if p < 4 else wf.at[k, z, :, at]
+        if dz == 0:
+            wf_own.append(near(block, to))
+        for d in (2,) if dz == 0 else (1, 3):
+            wf_in.append(remote(block, to, dz=d))
+
     def weights_y(p):
         wx_own[p].wait()
         for c in wx_in[p]:
             c.wait_recv()
-        wy_own.append(near(wx.at[p, :, y], wy.at[p, y]))
-        wy_in.append([remote(wx.at[p, :, (y + d) % 4], wy.at[p, y], dy=d) for d in (2, 1, 3)])
+        me, axis = (y, "dy") if p < 4 else (x, "dx")
+        wy_in[p] = [
+            remote(wx.at[p, :, (me + d) % 4], wy.at[p, me], **{axis: d}) for d in (2, 1, 3)
+        ]
+        weights_up(p, wx.at[p, :, me], me)
 
     def weights_z(p):
-        k, dz = pieces[p]
-        wy_own[p].wait()
-        for c in wy_in[p]:
+        me = y if p < 4 else x
+        for d, c in zip((2, 1, 3), wy_in[p]):
             c.wait_recv()
-        if dz == 0:
-            wf_own.append(near(wy.at[p], wf.at[k, z]))
-        for d in (2,) if dz == 0 else (1, 3):
-            wf_in.append(remote(wy.at[p], wf.at[k, z], dz=d))
+            weights_up(p, wy.at[p, (me + 4 - d) % 4], (me + 4 - d) % 4)
 
     axes = (("dx", "dy"), ("dy", "dx"))
     t1_own, t1_in, t2_in = {}, {}, {}
@@ -262,9 +290,11 @@
         for h in range(2):
             if j < 3:
                 t2_in[h, j].wait_recv()
-            bz_in[j, h] = remote(ty.at[h, j, :, 1], lhb.at[j, h, :, core], dz=1 + 2 * h)
-            a_in[j, h] = remote(ty.at[h, j, :, 0], lha.at[j, h, :, core], flip=True)
-            a_own[j, h] = near(ty.at[h, j, :, 0], lha.at[j, h, :, core])
+            half = ty.shape[3] // 2
+            near_half, far_half = (ty.at[h, j, :, pl.ds(i * half, half)] for i in range(2))
+            bz_in[j, h] = remote(far_half, lhb.at[j, h, :, core], dz=1 + 2 * h)
+            a_in[j, h] = remote(near_half, lha.at[j, h, :, core], flip=True)
+            a_own[j, h] = near(near_half, lha.at[j, h, :, core])
 
     def tokens_b(j):
         for h in range(2):
@@ -272,32 +302,37 @@
             b_in[j, h] = remote(lhb.at[j, h, :, core], lhb.at[j, h, :, core], flip=True)
 
     route()
+    weights_y(0)
+    weights_y(4)
     normalize()
     tile(0)
-    weights_y(0)
     tile(1)
+    weights_y(1)
+    weights_y(5)
     tile(2)
-    weights_y(1)
+    tile(3)
     weights_z(0)
-    tile(3)
+    weights_y(2)
     tile(4)
-    weights_y(2)
+    tile(5)
+    tile(6)
+    weights_y(3)
+    tile(7)
+    tokens_ready()
+    for j in (3, 0, 1, 2):
+        for h in range(2):
+            tokens_first(h, j)
     weights_z(1)
-    tile(5)
-    tokens_ready()
-    for j in range(4):
-        tokens_first(0, j)
-    for p in range(3, 6):
-        weights_y(p)
-        weights_z(p - 1)
-    for j in range(4):
-        tokens_first(1, j)
+    weights_z(2)
+    weights_z(4)
+    weights_z(3)
     weights_z(5)
-    for j in range(4):
+    tokens_second(0, 3)
+    tokens_second(1, 3)
+    tokens_third(3)
+    for j in range(3):
         tokens_second(0, j)
         tokens_second(1, j)
-    tokens_third(3)
-    tokens_third(0)
 
     pl.semaphore_wait(ready, len(peers))
     for c in wf_own:
@@ -352,12 +387,6 @@
                 remote(ref.at[j, h, d], ret.at[far, j, h, d], **{axes[h][0]: 4 - d})
             )
 
-    def second(ref, to, far, j, h):
-        if j < 3:
-            rq_in[far, j, h] = remote(ref.at[j, h], to.at[j, h], **{axes[h][1]: 4 - DYS[j]})
-        else:
-            home(ref, far, j, h)
-
     def finish(far, j):
         parts[far, j].wait_recv()
         ref = rb if far else ra
@@ -366,25 +395,28 @@
         for h in range(2):
             if far:
                 rz_in[j, h] = remote(rb.at[j, h], rz.at[j, h], dz=3 - 2 * h)
+            elif j < 3:
+                rq_in[j, h] = remote(ra.at[j, h], rya.at[j, h], **{axes[h][1]: 4 - DYS[j]})
             else:
-                second(ra, rya, 0, j, h)
+                home(ra, 0, j, h)
 
     def near_home(j):
         for h in range(2):
-            rq_in[0, j, h].wait_recv()
+            rq_in[j, h].wait_recv()
             home(rya, 0, j, h)
 
-    def far_second(j):
+    def far_home(j):
         for h in range(2):
             rz_in[j, h].wait_recv()
-            second(rz, ryb, 1, j, h)
-
-    def far_home(j):
-        for h in range(2):
-            rq_in[1, j, h].wait_recv()
-            home(ryb, 1, j, h)
+            if j == 3:
+                home(rz, 1, j, h)
+                continue
+            for d in (2, 1, 3, 0):
+                to = {axes[h][0]: (4 - d) % 4, axes[h][1]: 4 - DYS[j]}
+                out_in.append(remote(rz.at[j, h, d], ret.at[1, j, h, d], **to))
 
     expert(0, 3)
+    tokens_third(0)
     expert(0, 0)
     finish(0, 3)
     finish(0, 0)
@@ -401,21 +433,18 @@
     tokens_b(1)
     tokens_b(2)
     expert(1, 1)
+    near_home(1)
+    near_home(2)
     expert(1, 2)
     finish(1, 1)
     tokens_b(3)
     finish(1, 2)
-    near_home(1)
-    near_home(2)
-    far_second(0)
+    far_home(0)
     expert(1, 3)
     finish(1, 3)
-    far_second(1)
-    far_second(2)
-    far_home(0)
-    far_second(3)
     far_home(1)
     far_home(2)
+    far_home(3)
     for c in out_in:
         c.wait_recv()
     for c in out_own + written:
@@ -426,7 +455,7 @@
             c.wait_send()
 
 
-def exchange(group, picks, scales, tokens, gate, up, down):
+def exchange(group, picks, scales, gain, tokens, gate, up, down):
     model = tokens.shape[-1]
     total = tokens.size // model
     rows, width = gate.shape[-2:]
@@ -444,55 +473,52 @@
             served,
             served,
             served,
-            jax.ShapeDtypeStruct((2, 4, 4, 2, half, model), BF),
+            jax.ShapeDtypeStruct((2, 4, 4, 2 * half, model), BF),
             jax.ShapeDtypeStruct((8, total), F32),
         ),
-        in_specs=[vmem] * 3 + [hbm] * 4,
+        in_specs=[vmem] * 4 + [hbm] * 4,
         out_specs=(hbm,) * 5 + (vmem,),
         scratch_shapes=[
+            pltpu.VMEM((2, 2, 4, rows, width), F32),
+            pltpu.VMEM((6, 4, 4, rows, width), BF),
             pltpu.VMEM((6, 4, 4, rows, width), BF),
             pltpu.VMEM((6, 4, 4, rows, width), BF),
             pltpu.VMEM((3, 4, 4, 4, rows, width), BF),
-            pltpu.VMEM((2, 3, 4, 2, half, model), BF),
-            pltpu.VMEM((2, 4, 4, 2, half, model), BF),
+            pltpu.VMEM((2, 3, 4, 2 * half, model), BF),
+            pltpu.VMEM((2, 4, 4, 2 * half, model), BF),
             pltpu.VMEM((4, 2, 4, 2, half, model), BF),
             pltpu.VMEM((4, 2, 4, 2, half, model), BF),
             pltpu.VMEM((2,) + back, BF),
             pltpu.VMEM((2,) + back, BF),
-            pltpu.VMEM((18,) + back, BF),
-            pltpu.VMEM((experts * 2 * half, total), BF),
+            pltpu.VMEM((15,) + back, BF),
             pltpu.VMEM((experts, total), jnp.int32),
-            pltpu.VMEM((2, 2, 4, 4, 2, half, 512), BF),
-            pltpu.SemaphoreType.DMA((180,)),
-            pltpu.SemaphoreType.DMA((180,)),
-            pltpu.SemaphoreType.DMA((72,)),
+            pltpu.SemaphoreType.DMA((216,)),
+            pltpu.SemaphoreType.DMA((216,)),
+            pltpu.SemaphoreType.DMA((88,)),
             pltpu.SemaphoreType.REGULAR,
         ],
         compiler_params=pltpu.CompilerParams(
             collective_id=0, has_side_effects=True, vmem_limit_bytes=67_000_000
         ),
         name="exchange",
-    )(group, picks, scales, tokens, gate, up, down)
+    )(group, picks, scales, gain, tokens, gate, up, down)
 
 
 def local(
     tokens, norm_gain, gate_weight, up_weight, down_weight, group_pick, expert_pick, route_weight
 ):
     experts, rows, width = gate_weight.shape
-    scaled = norm_gain[None, :, None]
     split = (2, 4, 4, rows, width)
-    gate = (scaled * gate_weight).astype(BF).reshape(split)
-    up = (scaled * up_weight).astype(BF).reshape(split)
-    down = down_weight.astype(BF).reshape(split)
     tok_rows, model_width = tokens.shape
     returned, gate_new, up_new, down_new, _, table = exchange(
         group_pick[None, :],
         expert_pick.T,
         route_weight.T,
+        norm_gain[:, None],
         tokens.reshape(4, 2, 4, tok_rows // 32, model_width),
-        gate,
-        up,
-        down,
+        gate_weight.reshape(split),
+        up_weight.reshape(split),
+        down_weight.reshape(split),
     )
     served = [a.reshape(model_width, width) for a in (gate_new, up_new, down_new)]
     combined, *served = combine(

time: 225 us -> 211 us (0.938)
  Pallas kernels: 218 us -> 207 us
  other arithmetic: 6.46 us -> 0 us
    pallas_call x1, Pallas kernels: 203 us -> 192 us  [exchange(): pl.pallas_call(exchange_kernel, out_shape=(jax.ShapeDtypeStruct((2, 4) +...]
    convert_element_type x2 -> x0, other arithmetic: 6.46 us -> none  [the longest x1 3.51 us: local(): up = (scaled * up_weight).astype(BF).reshape(split)]
where the time goes in v5:
time: 211 us; the launch traced here: 210 us
  Pallas kernels  207 us (98%)
    pallas_call x1, Pallas kernels, exchange(): pl.pallas_call(exchange_kernel, out_shape=(jax.ShapeDtypeStruct((2, 4) +...  192 us
    pallas_call x1, Pallas kernels, combine(): pl.pallas_call(combine_kernel, grid=(steps,), out_shape=[jax.ShapeDtypeSt...  15.2 us

profile of v5, /device:TPU:1, one launch (start us, length us, event | category | flops | bytes accessed | tf_op | source)
XLA Modules:
  0.0 209.6 jit_solution(5598381306311902015)
XLA Ops:
  0.6 1.3 copy.12.gain
  2.0 192.2 %exchange.1 = (bf16[2,4,2,4,32,1536]{5,4,3,2,1,0:T(8,128)(2,1)}, bf16[4,4,4,48,384]{4,3,2,1,0:T(8,128)(2,1)}, bf16[4,4,4,48,384]{4,3,2,1,0:T(8,128)(2,1)}, bf16[...) custom-call(s32[1,1024]{1,0:T(1,128)} %bitcast.21, s32[2,1024]{1,0:T(2,128)} %bitcast.19, ...), custom_call_target="tpu_custom_call" | custom-call | tf_op jit(solution)/shard_map/exchange/pallas_call | solution.py:469
  194.2 15.2 %combine.1 = (bf16[1024,1536]{1,0:T(8,128)(2,1)}, bf16[3072,384]{1,0:T(8,128)(2,1)}, bf16[3072,384]{1,0:T(8,128)(2,1)}, bf16[3072,384]{1,0:T(8,128)(2,1)}) custom-call(f32[8,1024]{1,0:T(8,128)} %get-tuple-element.13.table_ref, bf16[2048,1536]{1,0:T(8,128)(2,1)} %bitcast.23, bf16[3072,384]{1,0:T(8,128)(2,1)} %bitcast.24, bf16[3072,384]{1,0:T(8,128)(2,1)} %bitcast.25, ...), custom_call_target="tpu_custom_call" | custom-call | flops 6442450944 | bytes 12582912 | tf_op jit(solution)/shard_map/combine/pallas_call | solution.py:53

commit v6 on v5

--- a/solution.py
+++ b/solution.py
@@ -47,7 +47,7 @@
 def combine(table, returned, served):
     lines, rows = table.shape
     slots, width = returned.shape
-    block = 512
+    block = 256
     steps = width // block
     lump = pl.BlockSpec((served[0].shape[0] // steps, served[0].shape[1]), lambda i: (i, 0))
     return pl.pallas_call(

time: 211 us -> 212 us (level)
  no operation moved by 1% of the time
where the time goes in v6:
time: 212 us; the launch traced here: 210 us
  Pallas kernels  208 us (98%)
    pallas_call x1, Pallas kernels, exchange(): pl.pallas_call(exchange_kernel, out_shape=(jax.ShapeDtypeStruct((2, 4) +...  192 us
    pallas_call x1, Pallas kernels, combine(): pl.pallas_call(combine_kernel, grid=(steps,), out_shape=[jax.ShapeDtypeSt...  16.1 us

profile of v6, /device:TPU:1, one launch (start us, length us, event | category | flops | bytes accessed | tf_op | source)
XLA Modules:
  0.0 210.5 jit_solution(982657070444371041)
XLA Ops:
  0.6 1.3 copy.12.gain
  2.0 192.2 %exchange.1 = (bf16[2,4,2,4,32,1536]{5,4,3,2,1,0:T(8,128)(2,1)}, bf16[4,4,4,48,384]{4,3,2,1,0:T(8,128)(2,1)}, bf16[4,4,4,48,384]{4,3,2,1,0:T(8,128)(2,1)}, bf16[...) custom-call(s32[1,1024]{1,0:T(1,128)} %bitcast.21, s32[2,1024]{1,0:T(2,128)} %bitcast.19, ...), custom_call_target="tpu_custom_call" | custom-call | tf_op jit(solution)/shard_map/exchange/pallas_call | solution.py:469
  194.2 16.1 %combine.1 = (bf16[1024,1536]{1,0:T(8,128)(2,1)}, bf16[3072,384]{1,0:T(8,128)(2,1)}, bf16[3072,384]{1,0:T(8,128)(2,1)}, bf16[3072,384]{1,0:T(8,128)(2,1)}) custom-call(f32[8,1024]{1,0:T(8,128)} %get-tuple-element.13.table_ref, bf16[2048,1536]{1,0:T(8,128)(2,1)} %bitcast.23, bf16[3072,384]{1,0:T(8,128)(2,1)} %bitcast.24, bf16[3072,384]{1,0:T(8,128)(2,1)} %bitcast.25, ...), custom_call_target="tpu_custom_call" | custom-call | flops 6442450944 | bytes 12582912 | tf_op jit(solution)/shard_map/combine/pallas_call | solution.py:53
